TPU v7x, 256 devices: a whole 4x4x8 slice. The times are simulated.
256 devices in a mesh: fs: 64 (over z, x, core), tp: 4 (over y).
Axes of the slice: x: 4, y: 4, z: 8, core: 2. Of those that a mesh axis runs over, the one named last changes fastest.
Arguments:
- tokens: bfloat16 [65536, 2048], P('fs', 'tp'), may hold values from -50 to 50
- norm_gain: float32 [2048], P('fs'), may hold values from 0.1 to 1.9
- gate_weight: float32 [2048, 2816], P('fs', 'tp'), may hold values from -0.125 to 0.125
- up_weight: float32 [2048, 2816], P('fs', 'tp'), may hold values from -0.125 to 0.125
- down_weight: float32 [2816, 2048], P('fs', 'tp'), may hold values from -0.109375 to 0.109375
Outputs:
- gate_sampler: bfloat16 [2048, 2816], P(None, 'tp')
- up_sampler: bfloat16 [2048, 2816], P(None, 'tp')
- down_sampler: bfloat16 [2816, 2048], P('tp')
- mixed: bfloat16 [65536, 2048], P('fs', 'tp')
All inputs are finite; a program needn't handle non-finite values.
Results may differ from a plain program's by a relative error of at most 0.0095.
Values may be sent and summed in bfloat16 or wider, within the bound.
A program may use at most 128 MiB of HBM per device.

v0:
```python
import jax
import jax.numpy as jnp
from jax import lax
from jax.sharding import Mesh
from jax.sharding import PartitionSpec as P

FS = ("fs_0", "fs_1", "fs_2")


norm_eps = 1e-06


def sent_together(arrays, axis, dim, along):
    ends, at = ([], 0)
    for a in arrays[:-1]:
        at += a.shape[along]
        ends.append(at)
    both = jnp.concatenate(arrays, axis=along)
    return tuple(jnp.split(lax.all_gather(both, axis, axis=dim, tiled=True), ends, axis=along))


def copy_for_each(array, axis):
    copies = jnp.broadcast_to(array, (lax.axis_size(axis), *array.shape))
    return lax.all_to_all(copies, axis, split_axis=0, concat_axis=0, tiled=True)


def in_order(parts, dim):
    lengths = list(parts.shape[1:])
    lengths[dim] *= parts.shape[0]
    return jnp.moveaxis(parts, 0, dim).reshape(lengths)


def gather_axes(array, axes, dim):
    far, near = axes
    first = copy_for_each(array, far)
    parts = jnp.swapaxes(copy_for_each(first, near), 0, 1)
    return in_order(parts.reshape(-1, *array.shape), dim)


def in_blocks(array, dim, size):
    lengths = array.shape
    parts = array.reshape(*lengths[:dim], size, lengths[dim] // size, *lengths[dim + 1 :])
    return jnp.moveaxis(parts, dim, 0)


def sum_at_owner(array, axis, dim):
    size = lax.axis_size(axis)
    parts = lax.all_to_all(in_blocks(array, dim, size), axis, 0, 0, tiled=True)
    return jnp.sum(parts.astype(jnp.float32), axis=0)


def shards(tokens, norm_gain, gate_weight, up_weight, down_weight):
    gate_local = (norm_gain[:, None] * gate_weight).astype(jnp.bfloat16)
    up_local = (norm_gain[:, None] * up_weight).astype(jnp.bfloat16)
    down_local = down_weight.astype(jnp.bfloat16)
    gathered = lax.all_gather(tokens, "tp", axis=1, tiled=True)
    floated = gathered.astype(jnp.float32)
    normed = (
        floated * lax.rsqrt(jnp.mean(floated * floated, axis=-1, keepdims=True) + norm_eps)
    ).astype(jnp.bfloat16)
    gate_sampler, up_sampler = sent_together((gate_local, up_local), FS, 0, 1)
    gate = jnp.dot(normed, gate_sampler, preferred_element_type=jnp.float32)
    up = jnp.dot(normed, up_sampler, preferred_element_type=jnp.float32)
    hidden = (jax.nn.silu(gate) * up).astype(jnp.bfloat16)
    down_columns = gather_axes(down_local, (("fs_0", "fs_1"), "fs_2"), 0)
    down_sampler = lax.all_to_all(down_columns, "tp", split_axis=0, concat_axis=1, tiled=True)
    terms = jnp.dot(hidden, down_sampler, preferred_element_type=jnp.float32)
    summed = sum_at_owner(terms.astype(jnp.bfloat16), "tp", 1)
    return (gate_sampler, up_sampler, down_sampler, summed.astype(jnp.bfloat16))


def solution(mesh):
    finer = Mesh(mesh.devices.reshape(8, 4, 2, mesh.shape["tp"]), ("fs_0", "fs_1", "fs_2", "tp"))
    return jax.shard_map(
        shards,
        mesh=finer,
        in_specs=(P(FS, "tp"), P(FS), P(FS, "tp"), P(FS, "tp"), P(FS, "tp")),
        out_specs=(P(None, "tp"), P(None, "tp"), P("tp", None), P(FS, "tp")),
        check_vma=False,
    )
```

profile of v0, /device:TPU:1, one launch (start us, length us, event | category | flops | bytes accessed | tf_op | source)
XLA Modules:
  0.0 239.7 jit_solution(16290443086123108635)
XLA Ops:
  7.2 0.0 all-gather.5.cloned.1.call-start
  7.2 0.7 all-gather.5.cloned.1.call-update
  7.9 0.0 all-gather.3.cloned.1.call-start
  7.9 1.0 multiply_convert_fusion.2
  9.0 0.7 pad_maximum_fusion
  9.7 0.0 all-gather.3.cloned.1.call-update
  9.7 0.9 convert_element_type.25
  10.6 0.2 broadcast_in_dim.4
  10.8 50.3 %all_to_all.34 = bf16[32,44,512]{2,1,0:T(8,128)(2,1)S(1)} all-to-all(bf16[32,44,512]{2,1,0:T(8,128)(2,1)S(1)} %broadcast_in_dim.4), channel_id=1, replica_groups=mesh['fs_0'=8,'fs_1'=4,'fs_2'=2,'tp'=4] {'fs_0','fs_1'}, dimensions={0} | all-to-all | bytes 2883584 | tf_op jit(solution)/shard_map/all_to_all | solution.py:24
  61.1 0.8 copy.21
  61.9 0.4 broadcast_in_dim.10
  62.3 8.4 %all_to_all.35 = bf16[2,32,44,512]{3,1,2,0:T(8,128)(2,1)S(1)} all-to-all(bf16[2,32,44,512]{3,1,2,0:T(8,128)(2,1)S(1)} %broadcast_in_dim.10), channel_id=1, replica_groups=mesh['fs_0'=8,'fs_1'=4,'fs_2'=2,'tp'=4] {'fs_2'}, dimensions={0} | all-to-all | bytes 5767168 | tf_op jit(solution)/shard_map/all_to_all | solution.py:24
  70.7 1.6 copy.22
  72.3 2.2 all_to_all.25
  74.5 38.1 %all_to_all.36 = bf16[4,704,512]{2,1,0:T(8,128)(2,1)S(1)} all-to-all(bf16[4,704,512]{2,1,0:T(8,128)(2,1)} %all_to_all.25), channel_id=1, replica_groups=mesh['fs_0'=8,'fs_1'=4,'fs_2'=2,'tp'=4] {'tp'}, dimensions={0} | all-to-all | bytes 5767168 | tf_op jit(solution)/shard_map/all_to_all | solution.py:66
  112.6 0.4 copy.28
  113.1 0.0 copy-start
  113.1 0.0 all-gather.5.cloned.1.call-done
  113.1 4.1 %fusion = f32[1024]{0:T(1024)S(1)} fusion(bf16[1024,2048]{1,0:T(8,128)(2,1)} %all-gather.5.cloned.1.call-done), kind=kLoop, calls=%fused_computation.2 | loop fusion | flops 6290432 | bytes 4198400 | tf_op jit(solution)/shard_map/reduce_sum | solution.py:59
  117.2 31.3 %all-gather.3.cloned.1.call-done = bf16[2048,1408]{1,0:T(8,128)(2,1)} async-done(((bf16[32,1408]{1,0:T(8,128)(2,1)}), bf16[2048,1408]{1,0:T(8,128)(2,1)}) %all-gather.3.cloned.1.call-update) | async-done | bytes 5767184 | tf_op jit(solution)/shard_map/all_gather | solution.py:19
  148.5 8.1 %fusion.3 = f32[1024,704]{0,1:T(8,128)} fusion(bf16[1024,2048]{1,0:T(8,128)(2,1)} %all-gather.5.cloned.1.call-done, f32[1024]{0:T(1024)S(1)} %add_rsqrt_fusion, bf16[2048,1408]{1,0:T(8,128)(2,1)} %all-gather.3.cloned.1.call-done), kind=kOutput, calls=%fused_computation.7 | convolution fusion | flops 2959081472 | bytes 10227712 | tf_op jit(solution)/shard_map/dot_general | solution.py:62
  156.6 0.0 copy-done
  156.6 13.9 %convolution_convert_fusion = bf16[1024,2048]{1,0:T(8,128)(2,1)} fusion(bf16[704,2048]{1,0:T(8,128)(2,1)S(1)} %bitcast.16, f32[1024,704]{0,1:T(8,128)} %fusion.3, bf16[1024,2048]{1,0:T(8,128)(2,1)} %all-gather.5.cloned.1.call-done, f32[1024]{0:T(1024)S(1)} %add_rsqrt_fusion, bf16[2048,1408]{1,0:T(8,128)(2,1)} %all-gather.3.cloned.1.call-done), kind=kOutput, calls=%fused_computation.5 | convolution fusion | flops 5918294016 | bytes 17305600 | tf_op jit(solution)/shard_map/dot_general | solution.py:67
  170.5 4.6 %copy.30 = bf16[128,4,8,512]{3,2,0,1:T(8,128)(2,1)} copy(bf16[128,4,8,512]{3,2,1,0:T(8,128)(2,1)} %bitcast.15) | data formatting | bytes 8388608 | tf_op jit(solution)/shard_map/reshape | solution.py:42
  175.2 5.1 %all-to-all-start.3 = ((bf16[4,1024,512]{2,1,0:T(8,128)(2,1)}), bf16[4,1024,512]{2,1,0:T(8,128)(2,1)}, u32[]{:S(2)}, u32[]{:S(2)}) async-start(bf16[4,1024,512]{2,1,0:T(8,128)(2,1)} %bitcast.12), calls=%async_computation.3 | async-start | bytes 8388608 | tf_op jit(solution)/shard_map/all_to_all | solution.py:48
  180.2 6.2 %fusion.11 = (bf16[2048,704]{1,0:T(8,128)(2,1)}, bf16[2048,704]{1,0:T(8,128)(2,1)S(1)}) fusion(bf16[2048,1408]{1,0:T(8,128)(2,1)} %all-gather.3.cloned.1.call-done), kind=kLoop, calls=%fused_computation.15 | loop fusion | bytes 11534336 | tf_op jit(solution)/shard_map/split | solution.py:19
  186.4 4.6 %copy.26 = bf16[2048,704]{0,1:T(8,128)(2,1)} copy(bf16[2048,704]{1,0:T(8,128)(2,1)} %get-tuple-element.12) | data formatting | bytes 5767168
  191.0 2.7 %copy.25 = bf16[2048,704]{0,1:T(8,128)(2,1)} copy(bf16[2048,704]{1,0:T(8,128)(2,1)S(1)} %get-tuple-element.13) | data formatting | bytes 5767168
  193.6 35.1 %all-to-all-done.3 = bf16[4,1024,512]{2,1,0:T(8,128)(2,1)} async-done(((bf16[4,1024,512]{2,1,0:T(8,128)(2,1)}), bf16[4,1024,512]{2,1,0:T(8,128)(2,1)}, u32[]{:S(2)}, u32[]{:S(2)}) %all-to-all-start.3) | async-done | bytes 4194336 | tf_op jit(solution)/shard_map/all_to_all | solution.py:48
  228.7 4.1 %reduce_sum.22 = bf16[1024,512]{1,0:T(8,128)(2,1)} reduce(bf16[4,1024,512]{2,1,0:T(8,128)(2,1)} %all-to-all-done.3, bf16[]{:T(256)} %constant.11.clone.1), dimensions={0}, to_apply=%region_1.2 | reduce | flops 1572864 | bytes 5242882 | tf_op jit(solution)/shard_map/reduce_sum | solution.py:49
  (1 shorter events, 0.0 us)
Async XLA Ops:
  7.2 105.9 %all-gather.5.cloned.1.call-start = ((), (), s32[]{:S(2)}) async-start(), calls=%async_computation.5 | async-start | bytes 5242880 | tf_op jit(solution)/shard_map/all_gather | solution.py:56
  7.9 140.6 %all-gather.3.cloned.1.call-start = ((), (), s32[]{:S(2)}) async-start(), calls=%async_computation.4 | async-start | bytes 5857280 | tf_op jit(solution)/shard_map/all_gather | solution.py:19
  113.1 43.6 %copy-start = (bf16[4,88,8,512]{3,2,0,1:T(8,128)(2,1)}, bf16[4,88,8,512]{3,2,0,1:T(8,128)(2,1)S(1)}, u32[]{:S(2)}) copy-start(bf16[4,88,8,512]{3,2,0,1:T(8,128)(2,1)S(1)} %copy.28) | copy-start | bytes 8650756
  175.2 53.6 %all-to-all-start.3 = ((bf16[4,1024,512]{2,1,0:T(8,128)(2,1)}), bf16[4,1024,512]{2,1,0:T(8,128)(2,1)}, u32[]{:S(2)}, u32[]{:S(2)}) async-start(bf16[4,1024,512]{2,1,0:T(8,128)(2,1)} %bitcast.12), calls=%async_computation.3 | async-start | bytes 8388608 | tf_op jit(solution)/shard_map/all_to_all | solution.py:48
Sparse Core Ops, SparseCore 0:
  9.8 54.3 all-gather.4
  67.5 80.9 all-gather.2
where the time goes:
time: 240 us
  blocking collectives  96.8 us (40%)
  waiting for transfers between devices  67.1 us (28%)
  local copies, waits for them, and re-layouts  23.6 us (10%)
  matrix products  22 us (9%)
  between operations  14.1 us (6%)
  other arithmetic  10.9 us (5%)
  starting transfers between devices  5.15 us (2%)
    all_to_all x2, blocking collectives, copy_for_each(): return lax.all_to_all(copies, axis, split_axis=0, concat_axis=0, tiled=True)  58.7 us
    all_to_all x1, blocking collectives, shards(): lax.all_to_all(down_columns, 'tp', split_axis=0, concat_axis=1, tiled=True)  38.1 us
    all_to_all x1, waiting for transfers between devices, sum_at_owner(): parts = lax.all_to_all(in_blocks(array, dim, size), axis, 0, 0, tiled=True)  35.1 us
    all_gather x1, waiting for transfers between devices, sent_together(): lax.all_gather(both, axis, axis=dim, tiled=True)  31.3 us
    dot_general x1, matrix products, shards(): terms = jnp.dot(hidden, down_sampler, preferred_element_type=jnp.float32)  13.9 us
    dot_general x1, matrix products, shards(): gate = jnp.dot(normed, gate_sampler, preferred_element_type=jnp.float32)  8.11 us
    unnamed x4, local copies, waits for them, and re-layouts  7.25 us
    split x1, local copies, waits for them, and re-layouts, sent_together(): jnp.split(lax.all_gather(both, axis, axis=dim, tiled=True), ends, axis=al...  6.16 us
  transfers between devices with their start and end apart: 3, of which 2 were waited for; matrix products, arithmetic and copies ran while one was open for 10% of the time, Pallas kernels for 0%

commit v1 on v0

v1 whole, which is shorter than its diff:
```python
import functools

import jax
import jax.numpy as jnp
from jax import lax
from jax.experimental import pallas as pl
from jax.experimental.pallas import tpu as pltpu
from jax.sharding import PartitionSpec as P

MESH = pl.DeviceIdType.MESH
BF = jnp.bfloat16
F32 = jnp.float32
NZ, NX, NC, NY = 8, 4, 2, 4
ROWS = 32
HID = 704
WIDE = 768
DROWS, COLS = 44, 512
D = 2048
CHUNK, CHUNKS = 256, 4
HALF = CHUNK // 2
EPS = 1e-06


def kernel(
    tok, gain, gw, uw, dw,
    go, uo, do, mo,
    xs, sg, sud, dsend, df, tmp, gst, ust, xn, hid, part, far, near, comb, sums, out,
    ps, pr, gxs, gxr, gzs, gzr, us, ur, uxs, uxr, ufs, ufr, ds_, dr, ts, tr, tfs, tfr, rs, rr, loc,
):
    f, y = lax.axis_index("fs"), lax.axis_index("tp")
    z, x, c = f // 8, (f // 2) % 4, f % 2
    za, zb = z // 2, z % 2

    def at(zz, xx, cc, yy):
        return ((zz * NX + xx) * NC + cc, yy)

    zp, zm = (z + 1) % NZ, (z + 7) % NZ
    xp, xm, x2 = (x + 1) % NX, (x + 3) % NX, (x + 2) % NX
    yp, ym, y2 = (y + 1) % NY, (y + 3) % NY, (y + 2) % NY
    z_next, z_prev = at(zp, x, c, y), at(zm, x, c, y)
    x_next, x_prev, x_far = at(z, xp, c, y), at(z, xm, c, y), at(z, x2, c, y)
    y_next, y_prev = at(z, x, c, yp), at(z, x, c, ym)
    twin = at(z, x, 1 - c, y)
    pz = 2 * y + zb
    swap = at(pz, x, c, za)
    moves = za != y

    def remote(src, dst, send, recv, device):
        return pltpu.make_async_remote_copy(
            src_ref=src, dst_ref=dst, send_sem=send, recv_sem=recv, device_id=device, device_id_type=MESH
        )

    eye = lax.broadcasted_iota(jnp.int32, (ROWS, ROWS), 0) == lax.broadcasted_iota(jnp.int32, (ROWS, ROWS), 1)
    scale = jnp.sum(jnp.where(eye, jnp.broadcast_to(gain[...], (ROWS, ROWS)), 0.0), axis=1, keepdims=True)
    tail = jnp.zeros((ROWS, WIDE - HID), F32)
    sg[z, x, c] = jnp.concatenate([scale * gw[...], tail], axis=1).astype(BF)
    sud[z, x, c, 0] = jnp.concatenate([scale * uw[...], tail], axis=1).astype(BF)
    low = jnp.concatenate([dw[pl.ds(ROWS, DROWS - ROWS), :], jnp.zeros((4, COLS), F32)], axis=0)
    right = jnp.concatenate([low[:, :256], low[:, 256:]], axis=0)
    packed = jnp.concatenate([dw[pl.ds(0, ROWS), :], right], axis=1).astype(BF)

    @pl.when(moves)
    def _():
        dsend[...] = packed

    @pl.when(jnp.logical_not(moves))
    def _():
        sud[z, x, c, 1] = packed

    df[pl.ds(HID, WIDE - HID), :] = jnp.zeros((WIDE - HID, D), BF)

    own_tokens = pltpu.make_async_copy(tok, xs.at[y], loc.at[0])
    own_tokens.start()

    barrier = pltpu.get_barrier_semaphore()
    for partner in (z_next, z_prev, x_next, x_prev, x_far, y_next, y_prev, twin):
        pl.semaphore_signal(barrier, inc=1, device_id=partner, device_id_type=MESH)

    @pl.when(moves)
    def _():
        pl.semaphore_signal(barrier, inc=1, device_id=swap, device_id_type=MESH)

    pl.semaphore_wait(barrier, 8 + moves.astype(jnp.int32))

    sends = []

    def go_(copy):
        copy.start()
        sends.append(copy)

    change = remote(dsend, sud.at[pz, x, c, 1], ps.at[0], pr.at[0], swap)

    @pl.when(moves)
    def _():
        change.start()

    def token_copy(way, j):
        rows = pl.ds(j * CHUNK, CHUNK)
        return remote(
            tok.at[rows], xs.at[y, rows], ts.at[way * CHUNKS + j], tr.at[way * CHUNKS + j], (y_next, y_prev)[way]
        )

    def token_forward(way, j):
        rows = pl.ds(j * CHUNK + way * HALF, HALF)
        block = xs.at[(ym, yp)[way], rows]
        return remote(block, block, tfs.at[way * CHUNKS + j], tfr.at[way * CHUNKS + j], (y_next, y_prev)[way])

    def token_pass(j):
        for way in range(2):
            token_copy(way, j).wait_recv()
            go_(token_forward(way, j))

    for j in range(CHUNKS):
        for way in range(2):
            go_(token_copy(way, j))

    own_gate = sg.at[z, x, c]
    gx = [remote(own_gate, own_gate, gxs.at[k], gxr.at[k], to) for k, to in enumerate((x_next, x_prev, x_far))]
    for copy in gx:
        go_(copy)

    @pl.when(moves)
    def _():
        change.wait_recv()

    def ud_z(way, k):
        block = sud.at[(z + (NZ - k if way == 0 else k)) % NZ, x, c]
        return remote(block, block, us.at[way * 4 + k], ur.at[way * 4 + k], (z_next, z_prev)[way])

    def g_z(way, k, h):
        block = sg.at[(z + (NZ - k if way == 0 else k)) % NZ, pl.ds(2 * h, 2), c]
        n = (way * 4 + k) * 2 + h
        return remote(block, block, gzs.at[n], gzr.at[n], (z_next, z_prev)[way])

    def ud_x(o, way):
        block = sud.at[(z + order[o]) % NZ, x, c]
        return remote(block, block, uxs.at[o * 2 + way], uxr.at[o * 2 + way], (x_next, x_prev)[way])

    def ud_f(o):
        way = turn[o]
        block = sud.at[(z + order[o]) % NZ, (xm, xp)[way], c]
        return remote(block, block, ufs.at[o], ufr.at[o], (x_next, x_prev)[way])

    def twin_copy(n, block):
        return remote(block, block, ds_.at[n], dr.at[n], twin)

    def g_twin(o, cc):
        return twin_copy(o, sg.at[(z + order[o]) % NZ, :, cc])

    def ud_twin(o, cc):
        return twin_copy(8 + o, sud.at[(z + order[o]) % NZ, :, cc])

    order = [0, 7, 1, 6, 2, 5, 3, 4]
    turn = [0, 0, 1, 0, 1, 0, 1, 1]

    def ud_arrived(o):
        for way in range(2):
            go_(ud_x(o, way))

    def x_pass(o):
        for way in range(2):
            ud_x(o, way).wait_recv()
        go_(ud_f(o))

    def x_end(o):
        ud_f(o).wait_recv()
        go_(ud_twin(o, c))

    for way in range(2):
        go_(ud_z(way, 0))
    ud_arrived(0)
    for copy in gx:
        copy.wait_recv()
    for h in range(2):
        for way in range(2):
            go_(g_z(way, 0, h))
    go_(g_twin(0, c))

    last = (4, 3)
    for k in range(1, 5):
        ways = [way for way in range(2) if k <= last[way]]
        for way in ways:
            ud_z(way, k - 1).wait_recv()
            if k < last[way]:
                go_(ud_z(way, k))
            ud_arrived(7 if k == 4 else 2 * k - 1 + way)
        for way in ways:
            for h in range(2):
                g_z(way, k - 1, h).wait_recv()
                if k < last[way]:
                    go_(g_z(way, k, h))
            go_(g_twin(7 if k == 4 else 2 * k - 1 + way, c))
        for o in [[0], [1, 2], [3, 4], [5, 6]][k - 1]:
            x_pass(o)
        for o in [[], [0], [1, 2], [3, 4]][k - 1]:
            x_end(o)
        token_pass(k - 1)
    x_pass(7)
    x_end(5)
    x_end(6)
    x_end(7)
    for o in range(8):
        g_twin(o, 1 - c).wait_recv()
        ud_twin(o, 1 - c).wait_recv()

    def assemble(n, carry):
        a, group = n // 4, n % 4
        for s in range(4):
            shard = sud[2 * a + group // 2, (group % 2) * 2 + s // 2, s % 2, 1].astype(F32)
            tmp[pl.ds(DROWS * s, ROWS), :] = shard[:, :COLS]
            at_row = DROWS * s + ROWS
            tmp[pl.ds(at_row, DROWS - ROWS), pl.ds(0, 256)] = shard[: DROWS - ROWS, COLS:]
            tmp[pl.ds(at_row, DROWS - ROWS), pl.ds(256, 256)] = shard[16 : 16 + DROWS - ROWS, COLS:]
        rows = pl.ds(pl.multiple_of(group * 176, 16), 176)
        df[rows, pl.ds(pl.multiple_of(a * COLS, COLS), COLS)] = tmp[...].astype(BF)
        return carry

    lax.fori_loop(0, 16, assemble, 0)
    own_tokens.wait()

    def message(kind, way, j):
        rows = {"far": 1 - way, "near": way, "comb": 1 - way}[kind]
        to_block = y2 if kind == "far" else (yp, ym)[way]
        src = sums.at[way, j] if kind == "comb" else part.at[j, to_block, pl.ds(rows * HALF, HALF)]
        dst = {"far": far, "near": near, "comb": comb}[kind].at[way, j]
        n = (("far", "near", "comb").index(kind) * 2 + way) * CHUNKS + j
        return remote(src, dst, rs.at[n], rr.at[n], (y_next, y_prev)[way])

    def compute(j):
        for way in range(2):
            token_forward(way, j).wait_recv()

        def normalise(t, carry):
            rows = pl.ds(pl.multiple_of(j * CHUNK + t * 32, 32), 32)
            total = jnp.zeros((32, 1), F32)
            for b in range(NY):
                v = xs[b, rows, :].astype(F32)
                total = total + jnp.sum(v * v, axis=1, keepdims=True)
            r = lax.rsqrt(total / D + EPS)
            for b in range(NY):
                v = xs[b, rows, :].astype(F32)
                xn[pl.ds(pl.multiple_of(t * 32, 32), 32), pl.ds(b * COLS, COLS)] = (v * r).astype(BF)
            return carry

        lax.fori_loop(0, CHUNK // 32, normalise, 0)

        def first(n, carry):
            cols = pl.ds(pl.multiple_of(n * 256, 256), 256)
            gate = jnp.dot(xn[...], sg[:, :, :, :, cols].reshape(D, 256), preferred_element_type=F32)
            up = jnp.dot(xn[...], sud[:, :, :, 0, :, cols].reshape(D, 256), preferred_element_type=F32)
            hid[:, cols] = (gate / (1.0 + jnp.exp(-gate)) * up).astype(BF)
            return carry

        lax.fori_loop(0, WIDE // 256, first, 0)

        def second(n, carry):
            b = (y + 2 + n) % NY
            cols = pl.ds(pl.multiple_of(b * COLS, COLS), COLS)
            part[j, b] = jnp.dot(hid[...], df[:, cols], preferred_element_type=F32).astype(BF)
            return carry

        lax.fori_loop(0, NY, second, 0)
        for kind in ("far", "near"):
            for way in range(2):
                message(kind, way, j).start()

    def combine(j):
        for way in range(2):
            message("far", way, j).wait_recv()
            rows = pl.ds((1 - way) * HALF, HALF)
            mine = part[j, (yp, ym)[way], rows, :].astype(F32)
            sums[way, j] = (mine + far[way, j].astype(F32)).astype(BF)
        for way in range(2):
            message("comb", way, j).start()

    def step(j, carry):
        @pl.when(j < CHUNKS)
        def _():
            compute(j)

        @pl.when(j > 0)
        def _():
            combine(j - 1)

        return carry

    lax.fori_loop(0, CHUNKS + 1, step, 0)

    def narrow(n, carry):
        zz, xx, cc = n // 8, (n // 2) % 4, n % 2
        gst[n] = sg[zz, xx, cc][:, :HID]
        ust[n] = sud[zz, xx, cc, 0][:, :HID]
        return carry

    lax.fori_loop(0, NZ * NX * NC, narrow, 0)
    weights = [
        pltpu.make_async_copy(gst, go, loc.at[1]),
        pltpu.make_async_copy(ust, uo, loc.at[2]),
        pltpu.make_async_copy(df.at[pl.ds(0, HID)], do, loc.at[3]),
    ]
    for copy in weights:
        copy.start()

    def out_copy(j):
        return pltpu.make_async_copy(out.at[j], mo.at[pl.ds(j * CHUNK, CHUNK)], loc.at[4 + j])

    def finish(j, carry):
        for way in range(2):
            message("near", way, j).wait_recv()
            message("comb", way, j).wait_recv()
        for half in range(2):
            rows = pl.ds(half * HALF, HALF)
            mine = part[j, y, rows, :].astype(F32)
            total = mine + near[half, j].astype(F32) + comb[1 - half, j].astype(F32)
            out[j, rows, :] = total.astype(BF)
        out_copy(j).start()
        return carry

    lax.fori_loop(0, CHUNKS, finish, 0)

    for copy in sends:
        copy.wait_send()

    @pl.when(moves)
    def _():
        change.wait_send()

    def drain(j, carry):
        for kind in ("far", "near", "comb"):
            for way in range(2):
                message(kind, way, j).wait_send()
        out_copy(j).wait()
        return carry

    lax.fori_loop(0, CHUNKS, drain, 0)
    for copy in weights:
        copy.wait()


def shards(tokens, norm_gain, gate_weight, up_weight, down_weight):
    vmem = functools.partial(pltpu.VMEM, dtype=BF)
    sem = pltpu.SemaphoreType.DMA
    anywhere = pl.BlockSpec(memory_space=pl.ANY)
    whole = pl.BlockSpec(memory_space=pltpu.VMEM)
    gate, up, down, mixed = pl.pallas_call(
        kernel,
        name="layer",
        out_shape=(
            jax.ShapeDtypeStruct((NZ * NX * NC, ROWS, HID), BF),
            jax.ShapeDtypeStruct((NZ * NX * NC, ROWS, HID), BF),
            jax.ShapeDtypeStruct((HID, D), BF),
            jax.ShapeDtypeStruct((CHUNK * CHUNKS, COLS), BF),
        ),
        in_specs=[anywhere, whole, whole, whole, whole],
        out_specs=(anywhere,) * 4,
        scratch_shapes=[
            vmem((NY, CHUNK * CHUNKS, COLS)),
            vmem((NZ, NX, NC, ROWS, WIDE)),
            vmem((NZ, NX, NC, 2, ROWS, WIDE)),
            vmem((ROWS, WIDE)),
            vmem((WIDE, D)),
            pltpu.VMEM((4 * DROWS, COLS), F32),
            vmem((NZ * NX * NC, ROWS, HID)),
            vmem((NZ * NX * NC, ROWS, HID)),
            vmem((CHUNK, D)),
            vmem((CHUNK, WIDE)),
            vmem((CHUNKS, NY, CHUNK, COLS)),
            vmem((2, CHUNKS, HALF, COLS)),
            vmem((2, CHUNKS, HALF, COLS)),
            vmem((2, CHUNKS, HALF, COLS)),
            vmem((2, CHUNKS, HALF, COLS)),
            vmem((CHUNKS, CHUNK, COLS)),
            sem((1,)), sem((1,)),
            sem((3,)), sem((3,)),
            sem((16,)), sem((16,)),
            sem((8,)), sem((8,)),
            sem((16,)), sem((16,)),
            sem((8,)), sem((8,)),
            sem((16,)), sem((16,)),
            sem((8,)), sem((8,)),
            sem((8,)), sem((8,)),
            sem((24,)), sem((24,)),
            sem((8,)),
        ],
        compiler_params=pltpu.CompilerParams(collective_id=0, has_side_effects=True, vmem_limit_bytes=44 * 2**20),
    )(tokens, norm_gain.reshape(1, ROWS), gate_weight, up_weight, down_weight)
    return (gate.reshape(D, HID), up.reshape(D, HID), down, mixed)


def solution(mesh):
    return jax.shard_map(
        shards,
        mesh=mesh,
        in_specs=(P("fs", "tp"), P("fs"), P("fs", "tp"), P("fs", "tp"), P("fs", "tp")),
        out_specs=(P(None, "tp"), P(None, "tp"), P("tp", None), P("fs", "tp")),
        check_vma=False,
    )
```

time: 240 us -> 112 us (0.47)
  blocking collectives: 96.8 us -> 0 us
  Pallas kernels: 0 us -> 93.8 us
  waiting for transfers between devices: 67.1 us -> 0 us
  matrix products: 22 us -> 0 us
  between operations: 14.1 us -> 0.67 us
  other arithmetic: 10.9 us -> 0 us
  local copies, waits for them, and re-layouts: 23.6 us -> 17.4 us
  starting transfers between devices: 5.15 us -> 0 us
    all_to_all x3 -> x0, blocking collectives: 96.8 us -> none  [the longest x2 58.7 us: copy_for_each(): return lax.all_to_all(copies, axis, split_axis=0, concat_axis=0, tiled=True)]
    pallas_call x0 -> x1, Pallas kernels: none -> 93.8 us  [shards(): pl.pallas_call(kernel, name='layer', out_shape=(jax.ShapeDtypeStruct((NZ...]
    all_to_all x1 -> x0, waiting for transfers between devices: 35.1 us -> none  [sum_at_owner(): parts = lax.all_to_all(in_blocks(array, dim, size), axis, 0, 0, tiled=True)]
    all_gather x2 -> x0, waiting for transfers between devices: 31.3 us -> none  [the longest x1 31.3 us: sent_together(): lax.all_gather(both, axis, axis=dim, tiled=True)]
    dot_general x2 -> x0, matrix products: 22 us -> none  [the longest x1 13.9 us: shards(): terms = jnp.dot(hidden, down_sampler, preferred_element_type=jnp.float32)]
    unnamed x4 -> x22, local copies, waits for them, and re-layouts: 7.25 us -> 17.4 us
    reduce_sum x2 -> x0, other arithmetic: 8.21 us -> none  [the longest x1 4.11 us: sum_at_owner(): return jnp.sum(parts.astype(jnp.float32), axis=0)]
    split x1 -> x0, local copies, waits for them, and re-layouts: 6.16 us -> none  [sent_together(): jnp.split(lax.all_gather(both, axis, axis=dim, tiled=True), ends, axis=al...]
  transfers between devices with their start and end apart: 3 -> 0, of which waited for: 2 -> 0; matrix products, arithmetic and copies ran while one was open for 10% -> 0% of each run, Pallas kernels for 0% -> 0%
where the time goes in v1:
time: 112 us
  Pallas kernels  93.8 us (84%)
  local copies, waits for them, and re-layouts  17.4 us (16%)
    pallas_call x1, Pallas kernels, shards(): pl.pallas_call(kernel, name='layer', out_shape=(jax.ShapeDtypeStruct((NZ...  93.8 us
    unnamed x22, local copies, waits for them, and re-layouts  17.4 us

profile of v1, /device:TPU:1, one launch (start us, length us, event | category | flops | bytes accessed | tf_op | source)
XLA Modules:
  0.0 111.9 jit_solution(16184131146220191692)
XLA Ops:
  0.6 0.0 copy-start.2
  0.6 1.2 %copy-done.2 = bf16[1024,512]{1,0:T(8,128)(2,1)S(1)} copy-done((bf16[1024,512]{1,0:T(8,128)(2,1)S(1)}, bf16[1024,512]{1,0:T(8,128)(2,1)}, u32[]{:S(2)}) %copy-start.2) | copy-done | bytes 1048600
  1.9 0.0 copy-start.5
  1.9 0.9 copy-done.5
  2.8 0.0 copy-start.6
  2.8 0.9 copy-done.6
  3.6 0.0 copy-start.7
  3.6 0.9 copy-done.7
  4.5 0.0 copy-start.8
  4.5 0.7 copy-done.8
  5.2 93.8 %layer.1 = (bf16[64,32,704]{2,1,0:T(8,128)(2,1)S(1)}, bf16[64,32,704]{2,1,0:T(8,128)(2,1)}, bf16[704,2048]{1,0:T(8,128)(2,1)S(1)}, bf16[1024,512]{1,0:T(8,128)(2,1)S(1)}) custom-call(bf16[1024,512]{1,0:T(8,128)(2,1)S(1)} %copy-done.2, f32[1,32]{1,0:T(1,128)S(1)} %bitcast.4, f32[32,704]{1,0:T(8,128)S(1)} %copy-done.5, f32[32,704]{1,0:T(8,128)S(1)} %copy-done.6, ...), custom_call_target="tpu_custom_call" | custom-call | tf_op jit(solution)/shard_map/layer/pallas_call | solution.py:345
  99.0 0.0 copy-start
  99.0 1.6 %copy-done = bf16[704,2048]{1,0:T(8,128)(2,1)} copy-done((bf16[704,2048]{1,0:T(8,128)(2,1)}, bf16[704,2048]{1,0:T(8,128)(2,1)S(1)}, u32[]{:S(2)}) %copy-start) | copy-done | bytes 2883608
  100.6 0.0 copy-start.3
  100.6 1.0 copy-done.3
  101.5 2.7 %copy.9 = bf16[2048,704]{0,1:T(8,128)(2,1)} copy(bf16[2048,704]{1,0:T(8,128)(2,1)S(1)} %bitcast.3) | data formatting | bytes 5767168
  104.2 0.0 copy-start.1
  104.2 4.7 %copy.10 = bf16[2048,704]{0,1:T(8,128)(2,1)} copy(bf16[2048,704]{1,0:T(8,128)(2,1)} %bitcast.5) | data formatting | bytes 5767168
  108.9 0.0 copy-done.1
  108.9 0.0 copy-start.4
  108.9 1.6 %copy.13 = bf16[704,2048]{1,0:T(8,128)(2,1)} copy(bf16[704,2048]{1,0:T(8,128)(2,1)S(1)} %copy-done.1) | data formatting | bytes 5767168
  110.5 0.4 copy-done.4
  110.9 1.0 copy.14
Async XLA Ops:
  0.6 1.2 %copy-start.2 = (bf16[1024,512]{1,0:T(8,128)(2,1)S(1)}, bf16[1024,512]{1,0:T(8,128)(2,1)}, u32[]{:S(2)}) copy-start(bf16[1024,512]{1,0:T(8,128)(2,1)} %tok.1) | copy-start | bytes 3145732
  1.9 0.9 copy-start.5
  2.8 0.9 copy-start.6
  3.6 0.9 copy-start.7
  4.5 0.7 copy-start.8
  99.0 1.6 %copy-start = (bf16[704,2048]{1,0:T(8,128)(2,1)}, bf16[704,2048]{1,0:T(8,128)(2,1)S(1)}, u32[]{:S(2)}) copy-start(bf16[704,2048]{1,0:T(8,128)(2,1)S(1)} %get-tuple-element.22) | copy-start | bytes 8650756
  100.6 1.0 copy-start.3
  104.2 4.7 %copy-start.1 = (bf16[704,2048]{1,0:T(8,128)(2,1)S(1)}, bf16[704,2048]{1,0:T(8,128)(2,1)}, u32[]{:S(2)}) copy-start(bf16[704,2048]{1,0:T(8,128)(2,1)} %copy-done) | copy-start | bytes 8650756
  108.9 2.0 %copy-start.4 = (bf16[1024,512]{1,0:T(8,128)(2,1)S(1)}, bf16[1024,512]{1,0:T(8,128)(2,1)}, u32[]{:S(2)}) copy-start(bf16[1024,512]{1,0:T(8,128)(2,1)} %copy-done.3) | copy-start | bytes 3145732

commit v2 on v1

v2 whole, which is shorter than its diff:
```python
import functools

import jax
import jax.numpy as jnp
from jax import lax
from jax.experimental import pallas as pl
from jax.experimental.pallas import tpu as pltpu
from jax.sharding import PartitionSpec as P

MESH = pl.DeviceIdType.MESH
BF = jnp.bfloat16
F32 = jnp.float32
NZ, NX, NC, NY = 8, 4, 2, 4
ROWS = 32
HID = 704
WIDE = 768
DROWS, COLS = 44, 512
D = 2048
CHUNK, CHUNKS = 256, 4
HALF = CHUNK // 2
EPS = 1e-06
VMEM_ALL = 67_043_328


def kernel(
    tok, gain_in, gw_in, uw_in, dw_in,
    go, uo, do, mo,
    gt, ut, df, out, gain, gw, uw, dw, xs, sg, sud, dsend, tmp, xn, hid, part, far, near, comb, sums,
    ps, pr, gxs, gxr, gzs, gzr, us, ur, uxs, uxr, ufs, ufr, ds_, dr, ts, tr, tfs, tfr, rs, rr, loc,
):
    f, y = lax.axis_index("fs"), lax.axis_index("tp")
    z, x, c = f // 8, (f // 2) % 4, f % 2
    za, zb = z // 2, z % 2

    def at(zz, xx, cc, yy):
        return ((zz * NX + xx) * NC + cc, yy)

    zp, zm = (z + 1) % NZ, (z + 7) % NZ
    xp, xm, x2 = (x + 1) % NX, (x + 3) % NX, (x + 2) % NX
    yp, ym, y2 = (y + 1) % NY, (y + 3) % NY, (y + 2) % NY
    z_next, z_prev = at(zp, x, c, y), at(zm, x, c, y)
    x_next, x_prev, x_far = at(z, xp, c, y), at(z, xm, c, y), at(z, x2, c, y)
    y_next, y_prev = at(z, x, c, yp), at(z, x, c, ym)
    twin = at(z, x, 1 - c, y)
    pz = 2 * y + zb
    swap = at(pz, x, c, za)
    moves = za != y

    def remote(src, dst, send, recv, device):
        return pltpu.make_async_remote_copy(
            src_ref=src, dst_ref=dst, send_sem=send, recv_sem=recv, device_id=device, device_id_type=MESH
        )

    own_tokens = pltpu.make_async_copy(tok, xs.at[y], loc.at[0])
    own = [
        pltpu.make_async_copy(src, dst, loc.at[1 + n])
        for n, (src, dst) in enumerate(((gain_in, gain), (gw_in, gw), (uw_in, uw), (dw_in, dw)))
    ]
    for copy in own:
        copy.start()
    own_tokens.start()

    barrier = pltpu.get_barrier_semaphore()
    for partner in (z_next, z_prev, x_next, x_prev, x_far, y_next, y_prev, twin):
        pl.semaphore_signal(barrier, inc=1, device_id=partner, device_id_type=MESH)

    @pl.when(moves)
    def _():
        pl.semaphore_signal(barrier, inc=1, device_id=swap, device_id_type=MESH)

    for copy in own:
        copy.wait()

    eye = lax.broadcasted_iota(jnp.int32, (ROWS, ROWS), 0) == lax.broadcasted_iota(jnp.int32, (ROWS, ROWS), 1)
    scale = jnp.sum(jnp.where(eye, jnp.broadcast_to(gain[...], (ROWS, ROWS)), 0.0), axis=1, keepdims=True)
    tail = jnp.zeros((ROWS, WIDE - HID), F32)
    sg[z, x, c] = jnp.concatenate([scale * gw[...], tail], axis=1).astype(BF)
    sud[z, x, c, 0] = jnp.concatenate([scale * uw[...], tail], axis=1).astype(BF)
    low = jnp.concatenate([dw[pl.ds(ROWS, DROWS - ROWS), :], jnp.zeros((4, COLS), F32)], axis=0)
    right = jnp.concatenate([low[:, :256], low[:, 256:]], axis=0)
    packed = jnp.concatenate([dw[pl.ds(0, ROWS), :], right], axis=1).astype(BF)

    @pl.when(moves)
    def _():
        dsend[...] = packed

    @pl.when(jnp.logical_not(moves))
    def _():
        sud[z, x, c, 1] = packed

    df[pl.ds(HID, WIDE - HID), :] = jnp.zeros((WIDE - HID, D), BF)

    with jax.named_scope("meet"):
        pl.semaphore_wait(barrier, 8 + moves.astype(jnp.int32))

    sends = []

    def go_(copy):
        copy.start()
        sends.append(copy)

    change = remote(dsend, sud.at[pz, x, c, 1], ps.at[0], pr.at[0], swap)

    @pl.when(moves)
    def _():
        change.start()

    def token_copy(way, j):
        rows = pl.ds(j * CHUNK, CHUNK)
        return remote(
            tok.at[rows], xs.at[y, rows], ts.at[way * CHUNKS + j], tr.at[way * CHUNKS + j], (y_next, y_prev)[way]
        )

    def token_forward(way, j):
        rows = pl.ds(j * CHUNK + way * HALF, HALF)
        block = xs.at[(ym, yp)[way], rows]
        return remote(block, block, tfs.at[way * CHUNKS + j], tfr.at[way * CHUNKS + j], (y_next, y_prev)[way])

    def token_pass(j):
        for way in range(2):
            token_copy(way, j).wait_recv()
            go_(token_forward(way, j))

    order = [0, 7, 1, 6, 2, 5, 3, 4]
    turn = [0, 0, 1, 0, 1, 0, 1, 1]
    last = (4, 3)

    def came(way, k):
        return (z + (NZ - k if way == 0 else k)) % NZ

    def place(way, k):
        return 7 if k == 4 else 2 * k - 1 + way

    def ud_z(q, way, k):
        block, n = sud.at[came(way, k), x, c, q], (q * 2 + way) * 4 + k
        return remote(block, block, us.at[n], ur.at[n], (z_next, z_prev)[way])

    def ud_x(q, o, way):
        block, n = sud.at[(z + order[o]) % NZ, x, c, q], (q * 8 + o) * 2 + way
        return remote(block, block, uxs.at[n], uxr.at[n], (x_next, x_prev)[way])

    def ud_f(q, o):
        way, n = turn[o], q * 8 + o
        block = sud.at[(z + order[o]) % NZ, (xm, xp)[way], c, q]
        return remote(block, block, ufs.at[n], ufr.at[n], (x_next, x_prev)[way])

    def g_z(way, k, e):
        block, n = sg.at[came(way, k), (x, xp, xm, x2)[e], c], (way * 4 + k) * 4 + e
        return remote(block, block, gzs.at[n], gzr.at[n], (z_next, z_prev)[way])

    def twin_copy(n, block):
        return remote(block, block, ds_.at[n], dr.at[n], twin)

    def g_twin(o, cc):
        return twin_copy(o, sg.at[(z + order[o]) % NZ, :, cc])

    def ud_twin(o, cc):
        return twin_copy(8 + o, sud.at[(z + order[o]) % NZ, :, cc])

    def ud_arrived(q, o):
        for way in range(2):
            go_(ud_x(q, o, way))

    def ud_round(q, k):
        for way in range(2):
            if k <= last[way]:
                ud_z(q, way, k - 1).wait_recv()
                if k < last[way]:
                    go_(ud_z(q, way, k))
                ud_arrived(q, place(way, k))

    def g_round(k, es):
        for e in es:
            for way in range(2):
                if k <= last[way]:
                    g_z(way, k - 1, e).wait_recv()
                    if k < last[way]:
                        go_(g_z(way, k, e))
        if es[-1] == 3:
            for way in range(2):
                if k <= last[way]:
                    go_(g_twin(place(way, k), c))

    def x_pass(*os):
        for o in os:
            for q in range(2):
                for way in range(2):
                    ud_x(q, o, way).wait_recv()
                go_(ud_f(q, o))

    def x_end(*os):
        for o in os:
            for q in range(2):
                ud_f(q, o).wait_recv()
            go_(ud_twin(o, c))

    own_gate = sg.at[z, x, c]
    gx = [remote(own_gate, own_gate, gxs.at[k], gxr.at[k], to) for k, to in enumerate((x_next, x_prev, x_far))]
    for way in range(2):
        go_(ud_z(0, way, 0))
    for copy in gx:
        go_(copy)
    for way in range(2):
        go_(g_z(way, 0, 0))
    ud_arrived(0, 0)
    for j in range(CHUNKS):
        for way in range(2):
            go_(token_copy(way, j))

    with jax.named_scope("change"):

        @pl.when(moves)
        def _():
            change.wait_recv()

    for way in range(2):
        go_(ud_z(1, way, 0))
    ud_arrived(1, 0)
    with jax.named_scope("gate_x"):
        for copy in gx:
            copy.wait_recv()
    for way in range(2):
        go_(g_z(way, 0, 1))
    go_(g_twin(0, c))

    with jax.named_scope("round_1"):
        ud_round(0, 1)
        ud_round(1, 1)
        for e in (2, 3):
            for way in range(2):
                go_(g_z(way, 0, e))
        x_pass(0)
    with jax.named_scope("round_2"):
        ud_round(0, 2)
        ud_round(1, 2)
        g_round(1, (0, 1))
        x_pass(1, 2)
        x_end(0)
        token_pass(0)
    with jax.named_scope("round_3"):
        ud_round(0, 3)
        ud_round(1, 3)
        g_round(1, (2, 3))
        x_pass(3, 4)
        x_end(1, 2)
    with jax.named_scope("round_4"):
        ud_round(0, 4)
        ud_round(1, 4)
        g_round(2, (0, 1))
        token_pass(1)
        x_pass(5, 6)
        x_end(3, 4)
    with jax.named_scope("round_5"):
        g_round(2, (2, 3))
        token_pass(2)
        x_pass(7)
    with jax.named_scope("round_6"):
        g_round(3, (0, 1, 2, 3))
        x_end(5, 6)
        token_pass(3)
    with jax.named_scope("round_7"):
        x_end(7)
        g_round(4, (0, 1, 2, 3))
    with jax.named_scope("tail_twin"):
        for o in range(8):
            g_twin(o, 1 - c).wait_recv()
            ud_twin(o, 1 - c).wait_recv()

    def assemble(n, carry):
        a, group = n // 4, n % 4
        for s in range(4):
            shard = sud[2 * a + group // 2, (group % 2) * 2 + s // 2, s % 2, 1].astype(F32)
            tmp[pl.ds(DROWS * s, ROWS), :] = shard[:, :COLS]
            at_row = DROWS * s + ROWS
            tmp[pl.ds(at_row, DROWS - ROWS), pl.ds(0, 256)] = shard[: DROWS - ROWS, COLS:]
            tmp[pl.ds(at_row, DROWS - ROWS), pl.ds(256, 256)] = shard[16 : 16 + DROWS - ROWS, COLS:]
        rows = pl.ds(pl.multiple_of(group * 176, 16), 176)
        df[rows, pl.ds(pl.multiple_of(a * COLS, COLS), COLS)] = tmp[...].astype(BF)
        return carry

    with jax.named_scope("assemble"):
        lax.fori_loop(0, 16, assemble, 0)
    own_tokens.wait()

    def message(kind, way, j):
        rows = {"far": 1 - way, "near": way, "comb": 1 - way}[kind]
        to_block = y2 if kind == "far" else (yp, ym)[way]
        src = sums.at[way, j] if kind == "comb" else part.at[j, to_block, pl.ds(rows * HALF, HALF)]
        dst = {"far": far, "near": near, "comb": comb}[kind].at[way, j]
        n = (("far", "near", "comb").index(kind) * 2 + way) * CHUNKS + j
        return remote(src, dst, rs.at[n], rr.at[n], (y_next, y_prev)[way])

    def compute(j):
        with jax.named_scope("wait_tokens"):
            for way in range(2):
                token_forward(way, j).wait_recv()

        def normalise(t, carry):
            rows = pl.ds(pl.multiple_of(j * CHUNK + t * 32, 32), 32)
            total = jnp.zeros((32, 1), F32)
            for b in range(NY):
                v = xs[b, rows, :].astype(F32)
                total = total + jnp.sum(v * v, axis=1, keepdims=True)
            r = lax.rsqrt(total / D + EPS)
            for b in range(NY):
                v = xs[b, rows, :].astype(F32)
                xn[pl.ds(pl.multiple_of(t * 32, 32), 32), pl.ds(b * COLS, COLS)] = (v * r).astype(BF)
            return carry

        with jax.named_scope("normalise"):
            lax.fori_loop(0, CHUNK // 32, normalise, 0)

        def first(n, carry):
            cols = pl.ds(pl.multiple_of(n * 256, 256), 256)
            gate = jnp.dot(xn[...], sg[:, :, :, :, cols].reshape(D, 256), preferred_element_type=F32)
            up = jnp.dot(xn[...], sud[:, :, :, 0, :, cols].reshape(D, 256), preferred_element_type=F32)
            hid[:, cols] = (gate / (1.0 + jnp.exp(-gate)) * up).astype(BF)
            return carry

        with jax.named_scope("first"):
            lax.fori_loop(0, WIDE // 256, first, 0)

        def second(n, carry):
            b = (y + 2 + n) % NY
            cols = pl.ds(pl.multiple_of(b * COLS, COLS), COLS)
            part[j, b] = jnp.dot(hid[...], df[:, cols], preferred_element_type=F32).astype(BF)
            return carry

        with jax.named_scope("second"):
            lax.fori_loop(0, NY, second, 0)
        for kind in ("far", "near"):
            for way in range(2):
                message(kind, way, j).start()

    def combine(j):
        for way in range(2):
            message("far", way, j).wait_recv()
            rows = pl.ds((1 - way) * HALF, HALF)
            mine = part[j, (yp, ym)[way], rows, :].astype(F32)
            sums[way, j] = (mine + far[way, j].astype(F32)).astype(BF)
        for way in range(2):
            message("comb", way, j).start()

    def step(j, carry):
        @pl.when(j < CHUNKS)
        def _():
            with jax.named_scope("compute"):
                compute(j)

        @pl.when(j > 0)
        def _():
            with jax.named_scope("combine"):
                combine(j - 1)

        return carry

    lax.fori_loop(0, CHUNKS + 1, step, 0)

    one = lax.broadcasted_iota(jnp.int32, (256, 256), 0) == lax.broadcasted_iota(jnp.int32, (256, 256), 1)
    unit = one.astype(F32).astype(BF)

    def turn_over(n, carry):
        q, cols = n % 4, pl.ds(pl.multiple_of(n // 4 * 256, 256), 256)
        to = pl.ds(pl.multiple_of(q * 512, 512), 512)
        for dst, src in ((gt, sg[pl.ds(2 * q, 2), :, :, :, cols]), (ut, sud[pl.ds(2 * q, 2), :, :, 0, :, cols])):
            dst[cols, to] = lax.dot_general(
                unit, src.reshape(512, 256), (((1,), (1,)), ((), ())), preferred_element_type=F32
            ).astype(BF)
        return carry

    with jax.named_scope("turn_over"):
        lax.fori_loop(0, 12, turn_over, 0)
    leaving = [
        pltpu.make_async_copy(src.at[pl.ds(0, HID)], dst, loc.at[5 + n])
        for n, (src, dst) in enumerate(((gt, go), (ut, uo), (df, do)))
    ]
    for copy in leaving:
        copy.start()

    def out_copy(j):
        rows = pl.ds(pl.multiple_of(j * CHUNK, CHUNK), CHUNK)
        return pltpu.make_async_copy(out.at[rows], mo.at[rows], loc.at[8 + j])

    def finish(j, carry):
        for way in range(2):
            message("near", way, j).wait_recv()
            message("comb", way, j).wait_recv()
        for half in range(2):
            rows = pl.ds(half * HALF, HALF)
            mine = part[j, y, rows, :].astype(F32)
            total = mine + near[half, j].astype(F32) + comb[1 - half, j].astype(F32)
            out[pl.ds(pl.multiple_of(j * CHUNK + half * HALF, HALF), HALF), :] = total.astype(BF)
        out_copy(j).start()
        return carry

    with jax.named_scope("finish"):
        lax.fori_loop(0, CHUNKS, finish, 0)

    for copy in sends:
        copy.wait_send()

    @pl.when(moves)
    def _():
        change.wait_send()

    def drain(j, carry):
        for kind in ("far", "near", "comb"):
            for way in range(2):
                message(kind, way, j).wait_send()
        out_copy(j).wait()
        return carry

    with jax.named_scope("drain"):
        lax.fori_loop(0, CHUNKS, drain, 0)
        for copy in leaving:
            copy.wait()


def hand_out(gt, ut, df, out, go, uo, do, mo, held, sem):
    n = 0
    moves = []
    for src, dst, rows in ((out, mo, 256), (gt, go, 176), (ut, uo, 176), (df, do, 176)):
        for k in range(4):
            part = pl.ds(k * rows, rows)
            slot = held.at[n, pl.ds(0, rows), pl.ds(0, src.shape[1])]
            moves.append(
                (
                    pltpu.make_async_copy(src.at[part], slot, sem.at[0, n]),
                    pltpu.make_async_copy(slot, dst.at[part], sem.at[1, n]),
                )
            )
            n += 1
    for come, _ in moves:
        come.start()
    for come, leave in moves:
        come.wait()
        leave.start()
    for _, leave in moves:
        leave.wait()


def shards(tokens, norm_gain, gate_weight, up_weight, down_weight):
    vmem = functools.partial(pltpu.VMEM, dtype=BF)
    sem = pltpu.SemaphoreType.DMA
    hbm = pl.BlockSpec(memory_space=pltpu.HBM)
    held = pl.pallas_call(
        kernel,
        name="layer",
        out_shape=(jax.ShapeDtypeStruct((HID, D), BF),) * 3 + (jax.ShapeDtypeStruct((CHUNK * CHUNKS, COLS), BF),),
        in_specs=[hbm] * 5,
        out_specs=(hbm,) * 4,
        scratch_shapes=[
            vmem((WIDE, D)),
            vmem((WIDE, D)),
            vmem((WIDE, D)),
            vmem((CHUNK * CHUNKS, COLS)),
            pltpu.VMEM((1, ROWS), F32),
            pltpu.VMEM((ROWS, HID), F32),
            pltpu.VMEM((ROWS, HID), F32),
            pltpu.VMEM((DROWS, COLS), F32),
            vmem((NY, CHUNK * CHUNKS, COLS)),
            vmem((NZ, NX, NC, ROWS, WIDE)),
            vmem((NZ, NX, NC, 2, ROWS, WIDE)),
            vmem((ROWS, WIDE)),
            pltpu.VMEM((4 * DROWS, COLS), F32),
            vmem((CHUNK, D)),
            vmem((CHUNK, WIDE)),
            vmem((CHUNKS, NY, CHUNK, COLS)),
            vmem((2, CHUNKS, HALF, COLS)),
            vmem((2, CHUNKS, HALF, COLS)),
            vmem((2, CHUNKS, HALF, COLS)),
            vmem((2, CHUNKS, HALF, COLS)),
            sem((1,)), sem((1,)),
            sem((3,)), sem((3,)),
            sem((32,)), sem((32,)),
            sem((16,)), sem((16,)),
            sem((32,)), sem((32,)),
            sem((16,)), sem((16,)),
            sem((16,)), sem((16,)),
            sem((8,)), sem((8,)),
            sem((8,)), sem((8,)),
            sem((24,)), sem((24,)),
            sem((12,)),
        ],
        compiler_params=pltpu.CompilerParams(collective_id=0, has_side_effects=True, vmem_limit_bytes=VMEM_ALL),
    )(tokens, norm_gain.reshape(1, ROWS), gate_weight, up_weight, down_weight)
    gate, up, down, mixed = pl.pallas_call(
        hand_out,
        name="hand_out",
        out_shape=(jax.ShapeDtypeStruct((HID, D), BF),) * 3 + (jax.ShapeDtypeStruct((CHUNK * CHUNKS, COLS), BF),),
        in_specs=[hbm] * 4,
        out_specs=(hbm,) * 4,
        scratch_shapes=[vmem((16, CHUNK, D)), sem((2, 16))],
        compiler_params=pltpu.CompilerParams(vmem_limit_bytes=VMEM_ALL),
    )(*held)
    return (gate.T, up.T, down, mixed)


def solution(mesh):
    return jax.shard_map(
        shards,
        mesh=mesh,
        in_specs=(P("fs", "tp"), P("fs"), P("fs", "tp"), P("fs", "tp"), P("fs", "tp")),
        out_specs=(P(None, "tp"), P(None, "tp"), P("tp", None), P("fs", "tp")),
        check_vma=False,
    )
```

time: 112 us -> 102 us (0.911)
  local copies, waits for them, and re-layouts: 17.4 us -> 0 us
  Pallas kernels: 93.8 us -> 101 us
    unnamed x22 -> x0, local copies, waits for them, and re-layouts: 17.4 us -> none
    pallas_call x1 -> x2, Pallas kernels: 93.8 us -> 101 us  [the longest x1 93.7 us: shards(): pl.pallas_call(kernel, name='layer', out_shape=(jax.ShapeDtypeStruct((HID...]
where the time goes in v2:
time: 102 us
  Pallas kernels  101 us (99%)
    pallas_call x1, Pallas kernels, shards(): pl.pallas_call(kernel, name='layer', out_shape=(jax.ShapeDtypeStruct((HID...  93.7 us
    pallas_call x1, Pallas kernels, shards(): pl.pallas_call(hand_out, name='hand_out', out_shape=(jax.ShapeDtypeStruct...  7.67 us

profile of v2, /device:TPU:1, one launch (start us, length us, event | category | flops | bytes accessed | tf_op | source)
XLA Modules:
  0.0 102.0 jit_solution(4538177980602930002)
XLA Ops:
  0.6 93.7 %layer.1 = (bf16[704,2048]{1,0:T(8,128)(2,1)}, bf16[704,2048]{1,0:T(8,128)(2,1)}, bf16[704,2048]{1,0:T(8,128)(2,1)}, bf16[1024,512]{1,0:T(8,128)(2,1)}) custom-call(bf16[1024,512]{1,0:T(8,128)(2,1)} %tok.1, f32[1,32]{1,0:T(1,128)} %bitcast.3, f32[32,704]{1,0:T(8,128)} %gw_in.1, f32[32,704]{1,0:T(8,128)} %uw_in.1, f32[44,512]{1,0:T(8,128)} %dw_in.1), custom_call_target="tpu_custom_call" | custom-call | tf_op jit(solution)/shard_map/layer/pallas_call | solution.py:446
  94.4 7.7 %hand_out.1 = (bf16[704,2048]{1,0:T(8,128)(2,1)}, bf16[704,2048]{1,0:T(8,128)(2,1)}, bf16[704,2048]{1,0:T(8,128)(2,1)}, bf16[1024,512]{1,0:T(8,128)(2,1)}) custom-call(bf16[704,2048]{1,0:T(8,128)(2,1)} %get-tuple-element.12.gt, bf16[704,2048]{1,0:T(8,128)(2,1)} %get-tuple-element.13.ut, bf16[704,2048]{1,0:T(8,128)(2,1)} %get-tuple-element.14.df, ...), custom_call_target="tpu_custom_call" | custom-call | tf_op jit(solution)/shard_map/hand_out/pallas_call | solution.py:487

commit v3 on v0

v3 whole, which is shorter than its diff:
```python
import functools

import jax
import jax.numpy as jnp
from jax import lax
from jax.experimental import pallas as pl
from jax.experimental.pallas import tpu as pltpu
from jax.sharding import PartitionSpec as P

MESH = pl.DeviceIdType.MESH
BF = jnp.bfloat16
F32 = jnp.float32
NZ, NX, NC, NY = 8, 4, 2, 4
ROWS = 32
HID = 704
WIDE = 768
DROWS, COLS = 44, 512
D = 2048
CHUNK, CHUNKS = 128, 8
PIECE, PIECES = 256, 4
HALF = CHUNK // 2
EPS = 1e-06
LIMIT = 38 * 2**20


def kernel(
    tok, gw, uw, dw,
    gt, ut, df, out,
    xs, sg, sud, dsend, tmp, xn, hid, part, far, got, sums,
    ps, pr, gxs, gxr, gzs, gzr, us, ur, uxs, uxr, ufs, ufr, ds_, dr, ts, tr, tfs, tfr, rs, rr, loc,
):
    f, y = lax.axis_index("fs"), lax.axis_index("tp")
    z, x, c = f // 8, (f // 2) % 4, f % 2
    za, zb = z // 2, z % 2

    def at(zz, xx, cc, yy):
        return ((zz * NX + xx) * NC + cc, yy)

    zp, zm = (z + 1) % NZ, (z + 7) % NZ
    xp, xm, x2 = (x + 1) % NX, (x + 3) % NX, (x + 2) % NX
    yp, ym, y2 = (y + 1) % NY, (y + 3) % NY, (y + 2) % NY
    z_next, z_prev = at(zp, x, c, y), at(zm, x, c, y)
    x_next, x_prev, x_far = at(z, xp, c, y), at(z, xm, c, y), at(z, x2, c, y)
    y_next, y_prev = at(z, x, c, yp), at(z, x, c, ym)
    twin = at(z, x, 1 - c, y)
    pz = 2 * y + zb
    swap = at(pz, x, c, za)
    moves = za != y

    def remote(src, dst, send, recv, device):
        return pltpu.make_async_remote_copy(
            src_ref=src, dst_ref=dst, send_sem=send, recv_sem=recv, device_id=device, device_id_type=MESH
        )

    own_tokens = pltpu.make_async_copy(tok, xs.at[y], loc.at[0])

    barrier = pltpu.get_barrier_semaphore()
    for partner in (z_next, z_prev, x_next, x_prev, x_far, y_next, y_prev, twin):
        pl.semaphore_signal(barrier, inc=1, device_id=partner, device_id_type=MESH)

    @pl.when(moves)
    def _():
        pl.semaphore_signal(barrier, inc=1, device_id=swap, device_id_type=MESH)

    with jax.named_scope("meet"):
        pl.semaphore_wait(barrier, 8 + moves.astype(jnp.int32))

    def token_copy(way, j):
        rows = pl.ds(j * PIECE, PIECE)
        return remote(tok.at[rows], xs.at[y, rows], ts.at[way], tr.at[way * PIECES + j], (y_next, y_prev)[way])

    def token_forward(way, j):
        rows = pl.ds(j * PIECE + way * (PIECE // 2), PIECE // 2)
        block = xs.at[(ym, yp)[way], rows]
        return remote(block, block, tfs.at[way], tfr.at[way * PIECES + j], (y_next, y_prev)[way])

    def token_pass(j):
        for way in range(2):
            token_copy(way, j).wait_recv()
            token_forward(way, j).start()

    for j in range(PIECES):
        for way in range(2):
            token_copy(way, j).start()
    own_tokens.start()

    head = dw[pl.ds(0, ROWS), :]
    low = jnp.concatenate([dw[pl.ds(ROWS, DROWS - ROWS), :].astype(F32), jnp.zeros((4, COLS), F32)], axis=0)
    right = jnp.concatenate([low[:, : COLS // 2], low[:, COLS // 2 :]], axis=0).astype(BF)

    @pl.when(moves)
    def _():
        dsend[:, pl.ds(0, COLS)] = head
        dsend[:, pl.ds(COLS, COLS // 2)] = right

    @pl.when(jnp.logical_not(moves))
    def _():
        sud[z, x, c, 1, :, pl.ds(0, COLS)] = head
        sud[z, x, c, 1, :, pl.ds(COLS, COLS // 2)] = right

    tail = jnp.zeros((ROWS, WIDE - HID), BF)
    sud[z, x, c, 0] = jnp.concatenate([uw[...], tail], axis=1)
    sg[z, x, c] = jnp.concatenate([gw[...], tail], axis=1)

    change = remote(dsend, sud.at[pz, x, c, 1], ps.at[0], pr.at[0], swap)

    @pl.when(moves)
    def _():
        change.start()

    order = [0, 7, 1, 6, 2, 5, 3, 4]
    last = (4, 3)

    def came(way, k):
        return (z + (NZ - k if way == 0 else k)) % NZ

    def place(way, k):
        return 7 if k == 4 else 2 * k - 1 + way

    def ud_z(q, way, k):
        block = sud.at[came(way, k), x, c, q]
        return remote(block, block, us.at[way], ur.at[(q * 2 + way) * 4 + k], (z_next, z_prev)[way])

    def ud_x(q, o, way):
        block = sud.at[(z + order[o]) % NZ, x, c, q]
        return remote(block, block, uxs.at[0], uxr.at[(q * 8 + o) * 2 + way], (x_next, x_prev)[way])

    def ud_f(q, o):
        block = sud.at[(z + order[o]) % NZ, (xm, xp)[q], c, q]
        return remote(block, block, ufs.at[0], ufr.at[q * 8 + o], (x_next, x_prev)[q])

    def g_z(way, k, e):
        block = sg.at[came(way, k), (x, xp, xm, x2)[e], c]
        return remote(block, block, gzs.at[way], gzr.at[(way * 4 + k) * 2 + e // 2], (z_next, z_prev)[way])

    def g_pair(way, k, h):
        block = sg.at[came(way, k), pl.ds(0, 2), c]
        return remote(block, block, gzs.at[way], gzr.at[(way * 4 + k) * 2 + h], (z_next, z_prev)[way])

    def g_twin(o):
        block = sg.at[(z + order[o]) % NZ, :, c]
        return remote(block, block, ds_.at[2], dr.at[2], twin)

    def ud_twin(q, o):
        block = sud.at[(z + order[o]) % NZ, :, c, q]
        return remote(block, block, ds_.at[q], dr.at[q], twin)

    def twins(n):
        block = sg.at[:, :, c] if n == 2 else sud.at[:, :, c, n]
        return remote(block, block, ds_.at[n], dr.at[n], twin)

    def ud_arrived(q, o):
        for way in range(2):
            ud_x(q, o, way).start()

    def ud_round(q, k):
        for way in range(2):
            if k <= last[way]:
                ud_z(q, way, k - 1).wait_recv()
                if k < last[way]:
                    ud_z(q, way, k).start()
                ud_arrived(q, place(way, k))

    def g_round(k, *hs):
        for h in hs:
            for way in range(2):
                if k <= last[way]:
                    g_pair(way, k - 1, h).wait_recv()
                    if k < last[way]:
                        for e in (2 * h, 2 * h + 1):
                            g_z(way, k, e).start()
                    if h == 1:
                        g_twin(place(way, k)).start()

    def x_pass(q, *os):
        for o in os:
            for way in (q, 1 - q):
                ud_x(q, o, way).wait_recv()
                if way == q:
                    ud_f(q, o).start()

    def x_end(q, *os):
        for o in os:
            ud_f(q, o).wait_recv()
            ud_twin(q, o).start()

    def g_x(k):
        block = sg.at[z, x, c]
        return remote(block, block, gxs.at[0], gxr.at[0], (x_next, x_prev, x_far)[k])

    three = sg.at[pl.ds(0, 3), x, c]
    all_gx = remote(three, three, gxs.at[0], gxr.at[0], x_next)

    for way in range(2):
        ud_z(0, way, 0).start()
    for k in range(3):
        g_x(k).start()
    ud_arrived(0, 0)
    for way in range(2):
        g_z(way, 0, 0).start()

    with jax.named_scope("change"):

        @pl.when(moves)
        def _():
            change.wait_recv()

    for way in range(2):
        ud_z(1, way, 0).start()
    ud_arrived(1, 0)
    with jax.named_scope("round_1"):
        ud_round(0, 1)
        all_gx.wait_recv()
        for e in (1, 2, 3):
            for way in range(2):
                g_z(way, 0, e).start()
        g_twin(0).start()
        x_pass(0, 0)
    with jax.named_scope("round_2"):
        ud_round(0, 2)
        ud_round(1, 1)
        x_pass(0, 1, 2)
        x_pass(1, 0)
        g_round(1, 0)
        x_end(0, 0)
        token_pass(0)
    with jax.named_scope("round_3"):
        ud_round(0, 3)
        ud_round(1, 2)
        x_pass(0, 3, 4)
        g_round(1, 1)
        x_pass(1, 1, 2)
        x_end(0, 1, 2)
        x_end(1, 0)
    with jax.named_scope("round_4"):
        ud_round(0, 4)
        ud_round(1, 3)
        x_pass(0, 5, 6)
        g_round(2, 0)
        token_pass(1)
        x_pass(1, 3, 4)
        x_end(0, 3, 4)
        x_end(1, 1, 2)
    with jax.named_scope("round_5"):
        ud_round(1, 4)
        x_pass(0, 7)
        g_round(2, 1)
        token_pass(2)
        x_pass(1, 5, 6)
        x_end(0, 5, 6)
        x_end(1, 3, 4)
    with jax.named_scope("round_6"):
        g_round(3, 0, 1)
        x_end(0, 7)
        x_pass(1, 7)
        token_pass(3)
    with jax.named_scope("round_7"):
        g_round(4, 0, 1)
        x_end(1, 5, 6)
    own_tokens.wait()

    def normalise(j):
        for k in range(PIECES):

            @pl.when(j == k * (PIECE // CHUNK))
            def _(k=k):
                for way in range(2):
                    token_forward(way, k).wait_recv()

        def rows_of(t, carry):
            rows = pl.ds(pl.multiple_of(j * CHUNK + t * 32, 32), 32)
            total = jnp.zeros((32, 1), F32)
            for b in range(NY):
                v = xs[b, rows, :].astype(F32)
                total = total + jnp.sum(v * v, axis=1, keepdims=True)
            r = lax.rsqrt(total / D + EPS)
            for b in range(NY):
                v = xs[b, rows, :].astype(F32)
                xn[pl.ds(pl.multiple_of(t * 32, 32), 32), pl.ds(b * COLS, COLS)] = (v * r).astype(BF)
            return carry

        lax.fori_loop(0, CHUNK // 32, rows_of, 0)

    def first():
        def columns(n, carry):
            cols = pl.ds(pl.multiple_of(n * 256, 256), 256)
            gate = jnp.dot(xn[...], sg[:, :, :, :, cols].reshape(D, 256), preferred_element_type=F32)
            up = jnp.dot(xn[...], sud[:, :, :, 0, :, cols].reshape(D, 256), preferred_element_type=F32)
            hid[:, cols] = (gate / (1.0 + jnp.exp(-gate)) * up).astype(BF)
            return carry

        lax.fori_loop(0, WIDE // 256, columns, 0)

    def message(kind, way, j):
        rows = {"far": 1 - way, "near": way, "comb": 1 - way}[kind]
        to_block = y2 if kind == "far" else (yp, ym)[way]
        src = sums.at[j, way] if kind == "comb" else part.at[j, to_block, pl.ds(rows * HALF, HALF)]
        dst = {"far": far.at[j, way], "near": got.at[j, way], "comb": got.at[j, 2 + way]}[kind]
        return remote(src, dst, rs.at[0], rr.at[j + (0 if kind == "far" else CHUNKS)], (y_next, y_prev)[way])

    def all_far(j):
        return remote(sums.at[j], far.at[j], rs.at[0], rr.at[j], y_next)

    def all_got(j):
        return remote(got.at[j], got.at[j], rs.at[0], rr.at[CHUNKS + j], y_next)

    def second(j):
        def block(n, carry):
            b = (y + 2 + n) % NY
            cols = pl.ds(pl.multiple_of(b * COLS, COLS), COLS)
            part[j, b] = jnp.dot(hid[...], df[:, cols], preferred_element_type=F32).astype(BF)

            @pl.when(n == 0)
            def _():
                for way in range(2):
                    message("far", way, j).start()

            return carry

        lax.fori_loop(0, NY, block, 0)
        for way in range(2):
            message("near", way, j).start()

    def combine(j):
        all_far(j).wait_recv()
        for way in range(2):
            mine = part[j, (yp, ym)[way], pl.ds((1 - way) * HALF, HALF), :].astype(F32)
            sums[j, way] = (mine + far[j, way].astype(F32)).astype(BF)
        for way in range(2):
            message("comb", way, j).start()

    with jax.named_scope("normalise_0"):
        normalise(0)
    with jax.named_scope("wait_up"):
        x_end(1, 7)
        twins(2).wait_recv()
        twins(0).wait_recv()
    with jax.named_scope("first_0"):
        first()
    with jax.named_scope("wait_down"):
        twins(1).wait_recv()

    def assemble(n, carry):
        a, group = n // 4, n % 4
        for s in range(4):
            shard = sud[2 * a + group // 2, (group % 2) * 2 + s // 2, s % 2, 1].astype(F32)
            tmp[pl.ds(DROWS * s, ROWS), :] = shard[:, :COLS]
            at_row = DROWS * s + ROWS
            tmp[pl.ds(at_row, DROWS - ROWS), pl.ds(0, 256)] = shard[: DROWS - ROWS, COLS:]
            tmp[pl.ds(at_row, DROWS - ROWS), pl.ds(256, 256)] = shard[16 : 16 + DROWS - ROWS, COLS:]
        rows = pl.ds(pl.multiple_of(group * 176, 16), 176)
        df[rows, pl.ds(pl.multiple_of(a * COLS, COLS), COLS)] = tmp[...].astype(BF)
        return carry

    with jax.named_scope("assemble"):
        df[pl.ds(HID, WIDE - HID), :] = jnp.zeros((WIDE - HID, D), BF)
        lax.fori_loop(0, 16, assemble, 0)

    one = lax.broadcasted_iota(jnp.int32, (256, 256), 0) == lax.broadcasted_iota(jnp.int32, (256, 256), 1)
    unit = one.astype(F32).astype(BF)

    def turn_over(n, carry):
        q, cols = n % 4, pl.ds(pl.multiple_of(n // 4 * 256, 256), 256)
        to = pl.ds(pl.multiple_of(q * 512, 512), 512)
        for dst, src in ((gt, sg[pl.ds(2 * q, 2), :, :, :, cols]), (ut, sud[pl.ds(2 * q, 2), :, :, 0, :, cols])):
            dst[cols, to] = lax.dot_general(
                unit, src.reshape(512, 256), (((1,), (1,)), ((), ())), preferred_element_type=F32
            ).astype(BF)
        return carry

    def step(j, carry):
        @pl.when(j < CHUNKS)
        def _():
            with jax.named_scope("second"):
                second(j)

        @pl.when(j > 0)
        def _():
            with jax.named_scope("combine"):
                combine(j - 1)

        @pl.when(j < CHUNKS - 1)
        def _():
            with jax.named_scope("first"):
                normalise(j + 1)
                first()

        @pl.when(jnp.logical_and(j >= 3, j < 7))
        def _():
            with jax.named_scope("turn_over"):
                lax.fori_loop(3 * j - 9, 3 * j - 6, turn_over, 0)

        return carry

    lax.fori_loop(0, CHUNKS + 1, step, 0)

    def finish(j, carry):
        all_got(j).wait_recv()
        for half in range(2):
            mine = part[j, y, pl.ds(half * HALF, HALF), :].astype(F32)
            total = mine + got[j, half].astype(F32) + got[j, 3 - half].astype(F32)
            out[pl.ds(pl.multiple_of(j * CHUNK + half * HALF, HALF), HALF), :] = total.astype(BF)
        return carry

    with jax.named_scope("finish"):
        lax.fori_loop(0, CHUNKS, finish, 0)

    with jax.named_scope("drain"):

        @pl.when(moves)
        def _():
            change.wait_send()

        all_gx.wait_send()
        for way, n in ((0, 4), (1, 3)):
            eight = sg.at[pl.ds(0, n), x]
            remote(eight, eight, us.at[way], ur.at[0], z_next).wait_send()
            four = sg.at[pl.ds(0, n), :, c]
            remote(four, four, gzs.at[way], gzr.at[0], z_next).wait_send()
            remote(tok, xs.at[y], ts.at[way], tr.at[0], y_next).wait_send()
            half = xs.at[0, pl.ds(0, PIECE * PIECES // 2)]
            remote(half, half, tfs.at[way], tfr.at[0], y_next).wait_send()
        block = sg.at[:, :, c]
        remote(block, block, uxs.at[0], uxr.at[0], x_next).wait_send()
        block = sg.at[pl.ds(0, 4), :, c]
        remote(block, block, ufs.at[0], ufr.at[0], x_next).wait_send()
        for n in range(3):
            twins(n).wait_send()
        block = xs.at[pl.ds(0, 3)]
        remote(block, block, rs.at[0], rr.at[0], y_next).wait_send()


def hand_out(gt, ut, df, out, go, uo, do, mo, sem):
    rows = pl.ds(0, HID)
    moved = ((gt.at[rows], go), (ut.at[rows], uo), (df.at[rows], do), (out, mo))
    copies = [pltpu.make_async_copy(src, dst, sem.at[n]) for n, (src, dst) in enumerate(moved)]
    for copy in copies:
        copy.start()
    for copy in copies:
        copy.wait()


def shards(tokens, norm_gain, gate_weight, up_weight, down_weight):
    vmem = functools.partial(pltpu.VMEM, dtype=BF)
    sem = pltpu.SemaphoreType.DMA
    hbm = pl.BlockSpec(memory_space=pltpu.HBM)
    held = pl.pallas_call(
        kernel,
        name="layer",
        out_shape=(jax.ShapeDtypeStruct((WIDE, D), BF),) * 3 + (jax.ShapeDtypeStruct((CHUNK * CHUNKS, COLS), BF),),
        in_specs=[hbm] + [pl.BlockSpec(memory_space=pltpu.VMEM)] * 3,
        out_specs=(pl.BlockSpec(memory_space=pltpu.VMEM),) * 4,
        scratch_shapes=[
            vmem((NY, CHUNK * CHUNKS, COLS)),
            vmem((NZ, NX, NC, ROWS, WIDE)),
            vmem((NZ, NX, NC, 2, ROWS, WIDE)),
            vmem((ROWS, WIDE)),
            pltpu.VMEM((4 * DROWS, COLS), F32),
            vmem((CHUNK, D)),
            vmem((CHUNK, WIDE)),
            vmem((CHUNKS, NY, CHUNK, COLS)),
            vmem((CHUNKS, 2, HALF, COLS)),
            vmem((CHUNKS, 4, HALF, COLS)),
            vmem((CHUNKS, 2, HALF, COLS)),
            sem((1,)), sem((1,)),
            sem((1,)), sem((1,)),
            sem((2,)), sem((16,)),
            sem((2,)), sem((16,)),
            sem((1,)), sem((32,)),
            sem((1,)), sem((16,)),
            sem((3,)), sem((3,)),
            sem((2,)), sem((2 * PIECES,)),
            sem((2,)), sem((2 * PIECES,)),
            sem((1,)), sem((2 * CHUNKS,)),
            sem((1,)),
        ],
        compiler_params=pltpu.CompilerParams(collective_id=0, has_side_effects=True, vmem_limit_bytes=LIMIT),
    )(
        tokens,
        (norm_gain[:, None] * gate_weight).astype(BF),
        (norm_gain[:, None] * up_weight).astype(BF),
        down_weight.astype(BF),
    )
    gate, up, down, mixed = pl.pallas_call(
        hand_out,
        name="hand_out",
        out_shape=(jax.ShapeDtypeStruct((HID, D), BF),) * 3 + (jax.ShapeDtypeStruct((CHUNK * CHUNKS, COLS), BF),),
        in_specs=[pl.BlockSpec(memory_space=pl.ANY)] * 4,
        out_specs=(hbm,) * 4,
        scratch_shapes=[sem((4,))],
        compiler_params=pltpu.CompilerParams(vmem_limit_bytes=2**20),
    )(*held)
    return (gate.T, up.T, down, mixed)


def solution(mesh):
    return jax.shard_map(
        shards,
        mesh=mesh,
        in_specs=(P("fs", "tp"), P("fs"), P("fs", "tp"), P("fs", "tp"), P("fs", "tp")),
        out_specs=(P(None, "tp"), P(None, "tp"), P("tp", None), P("fs", "tp")),
        check_vma=False,
    )
```

time: 240 us -> 96.1 us (0.40)
  blocking collectives: 96.8 us -> 0 us
  Pallas kernels: 0 us -> 92.1 us
  waiting for transfers between devices: 67.1 us -> 0 us
  local copies, waits for them, and re-layouts: 23.6 us -> 1.22 us
  matrix products: 22 us -> 0 us
  between operations: 14.1 us -> 0.65 us
  other arithmetic: 10.9 us -> 1.94 us
  starting transfers between devices: 5.15 us -> 0 us
    all_to_all x3 -> x0, blocking collectives: 96.8 us -> none  [the longest x2 58.7 us: copy_for_each(): return lax.all_to_all(copies, axis, split_axis=0, concat_axis=0, tiled=True)]
    pallas_call x0 -> x2, Pallas kernels: none -> 92.1 us  [the longest x1 88.4 us: shards(): pl.pallas_call(kernel, name='layer', out_shape=(jax.ShapeDtypeStruct((WID...]
    all_to_all x1 -> x0, waiting for transfers between devices: 35.1 us -> none  [sum_at_owner(): parts = lax.all_to_all(in_blocks(array, dim, size), axis, 0, 0, tiled=True)]
    all_gather x2 -> x0, waiting for transfers between devices: 31.3 us -> none  [the longest x1 31.3 us: sent_together(): lax.all_gather(both, axis, axis=dim, tiled=True)]
    dot_general x2 -> x0, matrix products: 22 us -> none  [the longest x1 13.9 us: shards(): terms = jnp.dot(hidden, down_sampler, preferred_element_type=jnp.float32)]
    reduce_sum x2 -> x0, other arithmetic: 8.21 us -> none  [the longest x1 4.11 us: sum_at_owner(): return jnp.sum(parts.astype(jnp.float32), axis=0)]
    split x1 -> x0, local copies, waits for them, and re-layouts: 6.16 us -> none  [sent_together(): jnp.split(lax.all_gather(both, axis, axis=dim, tiled=True), ends, axis=al...]
    unnamed x4 -> x2, local copies, waits for them, and re-layouts: 7.25 us -> 1.22 us
  transfers between devices with their start and end apart: 3 -> 0, of which waited for: 2 -> 0; matrix products, arithmetic and copies ran while one was open for 10% -> 0% of each run, Pallas kernels for 0% -> 0%
where the time goes in v3:
time: 96.1 us; the launch traced here: 96 us
  Pallas kernels  92.1 us (96%)
  other arithmetic  1.94 us (2%)
  local copies, waits for them, and re-layouts  1.22 us (1%)
    pallas_call x1, Pallas kernels, shards(): pl.pallas_call(kernel, name='layer', out_shape=(jax.ShapeDtypeStruct((WID...  88.4 us
    pallas_call x1, Pallas kernels, shards(): pl.pallas_call(hand_out, name='hand_out', out_shape=(jax.ShapeDtypeStruct...  3.77 us

profile of v3, /device:TPU:1, one launch (start us, length us, event | category | flops | bytes accessed | tf_op | source)
XLA Modules:
  0.0 96.0 jit_solution(9223933889321146073)
XLA Ops:
  0.6 0.9 convert_element_type.11.dw
  1.5 1.0 %multiply_convert_fusion = (bf16[32,704]{1,0:T(8,128)(2,1)S(1)}, bf16[32,704]{1,0:T(8,128)(2,1)S(1)}) fusion(f32[32,704]{1,0:T(8,128)} %param.8, f32[32]{0:T(128)} %param.6, f32[32,704]{1,0:T(8,128)} %param.7), kind=kLoop, calls=%fused_computation | loop fusion | flops 90112 | bytes 270464 | tf_op jit(solution)/shard_map/convert_element_type | solution.py:481
  2.6 0.0 copy-start
  2.6 1.2 %copy-done = bf16[1024,512]{1,0:T(8,128)(2,1)S(1)} copy-done((bf16[1024,512]{1,0:T(8,128)(2,1)S(1)}, bf16[1024,512]{1,0:T(8,128)(2,1)}, u32[]{:S(2)}) %copy-start) | copy-done | bytes 1048600
  3.8 88.4 %layer.1 = (bf16[768,2048]{1,0:T(8,128)(2,1)S(1)}, bf16[768,2048]{1,0:T(8,128)(2,1)S(1)}, bf16[768,2048]{1,0:T(8,128)(2,1)S(1)}, bf16[1024,512]{1,0:T(8,128)(2,1)S(1)}) custom-call(bf16[1024,512]{1,0:T(8,128)(2,1)S(1)} %copy-done, bf16[32,704]{1,0:T(8,128)(2,1)S(1)} %get-tuple-element.21.gw, bf16[32,704]{1,0:T(8,128)(2,1)S(1)} %get-tuple-element.20.uw, ...), custom_call_target="tpu_custom_call" | custom-call | tf_op jit(solution)/shard_map/layer/pallas_call | solution.py:447
  92.2 3.8 %hand_out.1 = (bf16[704,2048]{1,0:T(8,128)(2,1)}, bf16[704,2048]{1,0:T(8,128)(2,1)}, bf16[704,2048]{1,0:T(8,128)(2,1)}, bf16[1024,512]{1,0:T(8,128)(2,1)}) custom-call(bf16[768,2048]{1,0:T(8,128)(2,1)S(1)} %get-tuple-element.12.gt, bf16[768,2048]{1,0:T(8,128)(2,1)S(1)} %get-tuple-element.13.ut, bf16[768,2048]{1,0:T(8,128)(2,1)S(1)} %get-tuple-element.14.df, ...), custom_call_target="tpu_custom_call" | custom-call | tf_op jit(solution)/shard_map/hand_out/pallas_call | solution.py:484
Async XLA Ops:
  2.6 1.2 %copy-start = (bf16[1024,512]{1,0:T(8,128)(2,1)S(1)}, bf16[1024,512]{1,0:T(8,128)(2,1)}, u32[]{:S(2)}) copy-start(bf16[1024,512]{1,0:T(8,128)(2,1)} %tok.1) | copy-start | bytes 3145732

commit v4 on v3

--- a/solution.py
+++ b/solution.py
@@ -14,6 +14,7 @@
 ROWS = 32
 HID = 704
 WIDE = 768
+TILES = 11
 DROWS, COLS = 44, 512
 D = 2048
 CHUNK, CHUNKS = 128, 8
@@ -26,7 +27,7 @@
 def kernel(
     tok, gw, uw, dw,
     gt, ut, df, out,
-    xs, sg, sud, dsend, tmp, xn, hid, part, far, got, sums,
+    xs, sg, sud, ends, dsend, tmp, xn, hid, part, far, got, sums,
     ps, pr, gxs, gxr, gzs, gzr, us, ur, uxs, uxr, ufs, ufr, ds_, dr, ts, tr, tfs, tfr, rs, rr, loc,
 ):
     f, y = lax.axis_index("fs"), lax.axis_index("tp")
@@ -84,23 +85,28 @@
             token_copy(way, j).start()
     own_tokens.start()
 
-    head = dw[pl.ds(0, ROWS), :]
-    low = jnp.concatenate([dw[pl.ds(ROWS, DROWS - ROWS), :].astype(F32), jnp.zeros((4, COLS), F32)], axis=0)
-    right = jnp.concatenate([low[:, : COLS // 2], low[:, COLS // 2 :]], axis=0).astype(BF)
+    for ref, dst in ((uw, sud.at[z, x, c, 0]), (gw, sg.at[z, x, c])):
+        for t in range(5):
+            for r in range(2):
+                dst[2 * t + r] = ref[pl.ds(16 * r, 16), pl.ds(128 * t, 128)]
+        dst[10] = jnp.concatenate([ref[pl.ds(16 * r, 16), pl.ds(640, 64)] for r in range(2)], axis=1)
+
+    def own_down(dst):
+        for t in range(4):
+            for r in range(2):
+                dst[2 * t + r] = dw[pl.ds(16 * r, 16), pl.ds(128 * t, 128)]
+        low = dw[pl.ds(ROWS, DROWS - ROWS), :].astype(F32)
+        for p in range(3):
+            piece = [low[:, 128 * p : 128 * p + 128], low[4 * p : 4 * p + 4, 384:]]
+            dst[8 + p] = jnp.concatenate(piece, axis=0).astype(BF)
 
     @pl.when(moves)
     def _():
-        dsend[:, pl.ds(0, COLS)] = head
-        dsend[:, pl.ds(COLS, COLS // 2)] = right
+        own_down(dsend)
 
     @pl.when(jnp.logical_not(moves))
     def _():
-        sud[z, x, c, 1, :, pl.ds(0, COLS)] = head
-        sud[z, x, c, 1, :, pl.ds(COLS, COLS // 2)] = right
-
-    tail = jnp.zeros((ROWS, WIDE - HID), BF)
-    sud[z, x, c, 0] = jnp.concatenate([uw[...], tail], axis=1)
-    sg[z, x, c] = jnp.concatenate([gw[...], tail], axis=1)
+        own_down(sud.at[z, x, c, 1])
 
     change = remote(dsend, sud.at[pz, x, c, 1], ps.at[0], pr.at[0], swap)
 
@@ -109,7 +115,7 @@
         change.start()
 
     order = [0, 7, 1, 6, 2, 5, 3, 4]
-    last = (4, 3)
+    last = ((4, 3), (3, 4))
 
     def came(way, k):
         return (z + (NZ - k if way == 0 else k)) % NZ
@@ -155,18 +161,18 @@
 
     def ud_round(q, k):
         for way in range(2):
-            if k <= last[way]:
+            if k <= last[q][way]:
                 ud_z(q, way, k - 1).wait_recv()
-                if k < last[way]:
+                if k < last[q][way]:
                     ud_z(q, way, k).start()
                 ud_arrived(q, place(way, k))
 
     def g_round(k, *hs):
         for h in hs:
             for way in range(2):
-                if k <= last[way]:
+                if k < 4 or h == way:
                     g_pair(way, k - 1, h).wait_recv()
-                    if k < last[way]:
+                    if k < 3 or k == 3 and h == way:
                         for e in (2 * h, 2 * h + 1):
                             g_z(way, k, e).start()
                     if h == 1:
@@ -184,17 +190,22 @@
             ud_f(q, o).wait_recv()
             ud_twin(q, o).start()
 
-    def g_x(k):
+    def g_x(way):
         block = sg.at[z, x, c]
-        return remote(block, block, gxs.at[0], gxr.at[0], (x_next, x_prev, x_far)[k])
-
-    three = sg.at[pl.ds(0, 3), x, c]
-    all_gx = remote(three, three, gxs.at[0], gxr.at[0], x_next)
+        return remote(block, block, gxs.at[0], gxr.at[way], (x_next, x_prev)[way])
+
+    def g_far(way):
+        block = sg.at[z, (xm, xp)[way], c, (pl.ds(0, 6), pl.ds(6, 5))[way]]
+        return remote(block, block, gxs.at[0], gxr.at[2], (x_next, x_prev)[way])
+
+    def shards_of(n, send, recv):
+        block = sg.at[z, pl.ds(0, n), c]
+        return remote(block, block, send, recv, x_next)
 
     for way in range(2):
         ud_z(0, way, 0).start()
-    for k in range(3):
-        g_x(k).start()
+    for way in range(2):
+        g_x(way).start()
     ud_arrived(0, 0)
     for way in range(2):
         g_z(way, 0, 0).start()
@@ -209,53 +220,59 @@
         ud_z(1, way, 0).start()
     ud_arrived(1, 0)
     with jax.named_scope("round_1"):
+        for way in range(2):
+            g_x(way).wait_recv()
+            g_far(way).start()
         ud_round(0, 1)
-        all_gx.wait_recv()
-        for e in (1, 2, 3):
+        for e in (1, 2):
             for way in range(2):
                 g_z(way, 0, e).start()
+        x_pass(0, 0)
+        shards_of(1, gxs.at[0], gxr.at[2]).wait_recv()
+        for way in range(2):
+            g_z(way, 0, 3).start()
         g_twin(0).start()
-        x_pass(0, 0)
     with jax.named_scope("round_2"):
         ud_round(0, 2)
+        g_round(1, 0)
         ud_round(1, 1)
         x_pass(0, 1, 2)
+        g_round(1, 1)
         x_pass(1, 0)
-        g_round(1, 0)
-        x_end(0, 0)
         token_pass(0)
     with jax.named_scope("round_3"):
         ud_round(0, 3)
+        g_round(2, 0)
         ud_round(1, 2)
         x_pass(0, 3, 4)
-        g_round(1, 1)
+        g_round(2, 1)
         x_pass(1, 1, 2)
+        x_end(0, 0)
+    with jax.named_scope("round_4"):
+        ud_round(0, 4)
+        g_round(3, 0)
+        ud_round(1, 3)
+        x_pass(0, 5, 6)
+        g_round(3, 1)
+        token_pass(1)
+        x_pass(1, 3, 4)
         x_end(0, 1, 2)
         x_end(1, 0)
-    with jax.named_scope("round_4"):
-        ud_round(0, 4)
-        ud_round(1, 3)
-        x_pass(0, 5, 6)
-        g_round(2, 0)
-        token_pass(1)
-        x_pass(1, 3, 4)
-        x_end(0, 3, 4)
-        x_end(1, 1, 2)
     with jax.named_scope("round_5"):
         ud_round(1, 4)
         x_pass(0, 7)
-        g_round(2, 1)
+        g_round(4, 0, 1)
         token_pass(2)
+        x_end(0, 3, 4)
         x_pass(1, 5, 6)
+        x_end(1, 1, 2)
+    with jax.named_scope("round_6"):
         x_end(0, 5, 6)
-        x_end(1, 3, 4)
-    with jax.named_scope("round_6"):
-        g_round(3, 0, 1)
-        x_end(0, 7)
         x_pass(1, 7)
         token_pass(3)
+        x_end(1, 3, 4)
     with jax.named_scope("round_7"):
-        g_round(4, 0, 1)
+        x_end(0, 7)
         x_end(1, 5, 6)
     own_tokens.wait()
 
@@ -281,15 +298,35 @@
 
         lax.fori_loop(0, CHUNK // 32, rows_of, 0)
 
+    def columns(q, n, pairs):
+        zs, rows = pl.ds(2 * pairs.start, 2 * pairs.size), pairs.size * D // 4
+        halves = []
+        for t in (2 * n, 2 * n + 1):
+            pair = pl.ds(2 * t, 2)
+            if t == 5:
+                half = ends[q, zs]
+            elif q == 0:
+                half = sud[zs, :, :, 0, pair]
+            else:
+                half = sg[zs, :, :, pair]
+            halves.append(half.reshape(rows, 128))
+        return jnp.concatenate(halves, axis=1)
+
     def first():
-        def columns(n, carry):
-            cols = pl.ds(pl.multiple_of(n * 256, 256), 256)
-            gate = jnp.dot(xn[...], sg[:, :, :, :, cols].reshape(D, 256), preferred_element_type=F32)
-            up = jnp.dot(xn[...], sud[:, :, :, 0, :, cols].reshape(D, 256), preferred_element_type=F32)
-            hid[:, cols] = (gate / (1.0 + jnp.exp(-gate)) * up).astype(BF)
-            return carry
-
-        lax.fori_loop(0, WIDE // 256, columns, 0)
+        for n in range(3):
+            gate = jnp.dot(xn[...], columns(1, n, pl.ds(0, 4)), preferred_element_type=F32)
+            up = jnp.dot(xn[...], columns(0, n, pl.ds(0, 4)), preferred_element_type=F32)
+            hid[:, pl.ds(256 * n, 256)] = (gate / (1.0 + jnp.exp(-gate)) * up).astype(BF)
+
+    def spread(n, carry):
+        left = lax.broadcasted_iota(jnp.int32, (NX, NC, 16, 128), 3) < 64
+        for q, tile in ((0, sud[n, :, :, 0, 10]), (1, sg[n, :, :, 10])):
+            tile = tile.astype(F32)
+            flat = tile.reshape(NX * NC * 16, 128)
+            turned = pltpu.roll(flat, 64, 1).reshape(NX, NC, 16, 128)
+            ends[q, n, :, :, 0] = jnp.where(left, tile, 0.0).astype(BF)
+            ends[q, n, :, :, 1] = jnp.where(left, turned, 0.0).astype(BF)
+        return carry
 
     def message(kind, way, j):
         rows = {"far": 1 - way, "near": way, "comb": 1 - way}[kind]
@@ -336,6 +373,7 @@
         twins(2).wait_recv()
         twins(0).wait_recv()
     with jax.named_scope("first_0"):
+        lax.fori_loop(0, NZ, spread, 0)
         first()
     with jax.named_scope("wait_down"):
         twins(1).wait_recv()
@@ -343,11 +381,15 @@
     def assemble(n, carry):
         a, group = n // 4, n % 4
         for s in range(4):
-            shard = sud[2 * a + group // 2, (group % 2) * 2 + s // 2, s % 2, 1].astype(F32)
-            tmp[pl.ds(DROWS * s, ROWS), :] = shard[:, :COLS]
-            at_row = DROWS * s + ROWS
-            tmp[pl.ds(at_row, DROWS - ROWS), pl.ds(0, 256)] = shard[: DROWS - ROWS, COLS:]
-            tmp[pl.ds(at_row, DROWS - ROWS), pl.ds(256, 256)] = shard[16 : 16 + DROWS - ROWS, COLS:]
+            shard = sud.at[2 * a + group // 2, (group % 2) * 2 + s // 2, s % 2, 1]
+            at_row = DROWS * s
+            for t in range(4):
+                for r in range(2):
+                    tmp[pl.ds(at_row + 16 * r, 16), pl.ds(128 * t, 128)] = shard[2 * t + r].astype(F32)
+            for p in range(3):
+                piece = shard[8 + p].astype(F32)
+                tmp[pl.ds(at_row + ROWS, 12), pl.ds(128 * p, 128)] = piece[:12]
+                tmp[pl.ds(at_row + ROWS + 4 * p, 4), pl.ds(384, 128)] = piece[12:]
         rows = pl.ds(pl.multiple_of(group * 176, 16), 176)
         df[rows, pl.ds(pl.multiple_of(a * COLS, COLS), COLS)] = tmp[...].astype(BF)
         return carry
@@ -359,14 +401,13 @@
     one = lax.broadcasted_iota(jnp.int32, (256, 256), 0) == lax.broadcasted_iota(jnp.int32, (256, 256), 1)
     unit = one.astype(F32).astype(BF)
 
-    def turn_over(n, carry):
-        q, cols = n % 4, pl.ds(pl.multiple_of(n // 4 * 256, 256), 256)
-        to = pl.ds(pl.multiple_of(q * 512, 512), 512)
-        for dst, src in ((gt, sg[pl.ds(2 * q, 2), :, :, :, cols]), (ut, sud[pl.ds(2 * q, 2), :, :, 0, :, cols])):
-            dst[cols, to] = lax.dot_general(
-                unit, src.reshape(512, 256), (((1,), (1,)), ((), ())), preferred_element_type=F32
-            ).astype(BF)
-        return carry
+    def turn_over(quarter):
+        to = pl.ds(pl.multiple_of(quarter * 512, 512), 512)
+        for n in range(3):
+            for q, dst in ((0, ut), (1, gt)):
+                dst[pl.ds(256 * n, 256), to] = lax.dot_general(
+                    unit, columns(q, n, pl.ds(quarter, 1)), (((1,), (1,)), ((), ())), preferred_element_type=F32
+                ).astype(BF)
 
     def step(j, carry):
         @pl.when(j < CHUNKS)
@@ -388,7 +429,7 @@
         @pl.when(jnp.logical_and(j >= 3, j < 7))
         def _():
             with jax.named_scope("turn_over"):
-                lax.fori_loop(3 * j - 9, 3 * j - 6, turn_over, 0)
+                turn_over(j - 3)
 
         return carry
 
@@ -411,12 +452,12 @@
         def _():
             change.wait_send()
 
-        all_gx.wait_send()
-        for way, n in ((0, 4), (1, 3)):
-            eight = sg.at[pl.ds(0, n), x]
-            remote(eight, eight, us.at[way], ur.at[0], z_next).wait_send()
-            four = sg.at[pl.ds(0, n), :, c]
-            remote(four, four, gzs.at[way], gzr.at[0], z_next).wait_send()
+        shards_of(3, gxs.at[0], gxr.at[0]).wait_send()
+        for way in range(2):
+            block = sg.at[pl.ds(0, 7), x, c]
+            remote(block, block, us.at[way], ur.at[0], z_next).wait_send()
+            block = sg.at[pl.ds(0, 7), x]
+            remote(block, block, gzs.at[way], gzr.at[0], z_next).wait_send()
             remote(tok, xs.at[y], ts.at[way], tr.at[0], y_next).wait_send()
             half = xs.at[0, pl.ds(0, PIECE * PIECES // 2)]
             remote(half, half, tfs.at[way], tfr.at[0], y_next).wait_send()
@@ -452,9 +493,10 @@
         out_specs=(pl.BlockSpec(memory_space=pltpu.VMEM),) * 4,
         scratch_shapes=[
             vmem((NY, CHUNK * CHUNKS, COLS)),
-            vmem((NZ, NX, NC, ROWS, WIDE)),
-            vmem((NZ, NX, NC, 2, ROWS, WIDE)),
-            vmem((ROWS, WIDE)),
+            vmem((NZ, NX, NC, TILES, 16, 128)),
+            vmem((NZ, NX, NC, 2, TILES, 16, 128)),
+            vmem((2, NZ, NX, NC, 2, 16, 128)),
+            vmem((TILES, 16, 128)),
             pltpu.VMEM((4 * DROWS, COLS), F32),
             vmem((CHUNK, D)),
             vmem((CHUNK, WIDE)),
@@ -463,7 +505,7 @@
             vmem((CHUNKS, 4, HALF, COLS)),
             vmem((CHUNKS, 2, HALF, COLS)),
             sem((1,)), sem((1,)),
-            sem((1,)), sem((1,)),
+            sem((1,)), sem((3,)),
             sem((2,)), sem((16,)),
             sem((2,)), sem((16,)),
             sem((1,)), sem((32,)),

time: 96.1 us -> 91 us (0.947)
  Pallas kernels: 92.1 us -> 87 us
    pallas_call x1, Pallas kernels: 88.4 us -> 83.2 us  [shards(): pl.pallas_call(kernel, name='layer', out_shape=(jax.ShapeDtypeStruct((WID...]
where the time goes in v4:
time: 91 us; the launch traced here: 90.8 us
  Pallas kernels  87 us (96%)
  other arithmetic  1.94 us (2%)
  local copies, waits for them, and re-layouts  1.22 us (1%)
    pallas_call x1, Pallas kernels, shards(): pl.pallas_call(kernel, name='layer', out_shape=(jax.ShapeDtypeStruct((WID...  83.2 us
    pallas_call x1, Pallas kernels, shards(): pl.pallas_call(hand_out, name='hand_out', out_shape=(jax.ShapeDtypeStruct...  3.77 us

profile of v4, /device:TPU:1, one launch (start us, length us, event | category | flops | bytes accessed | tf_op | source)
XLA Modules:
  0.0 90.8 jit_solution(7516829780273658878)
XLA Ops:
  0.6 0.9 convert_element_type.11.dw
  1.5 1.0 %multiply_convert_fusion = (bf16[32,704]{1,0:T(8,128)(2,1)S(1)}, bf16[32,704]{1,0:T(8,128)(2,1)S(1)}) fusion(f32[32,704]{1,0:T(8,128)} %param.8, f32[32]{0:T(128)} %param.6, f32[32,704]{1,0:T(8,128)} %param.7), kind=kLoop, calls=%fused_computation | loop fusion | flops 90112 | bytes 270464 | tf_op jit(solution)/shard_map/convert_element_type | solution.py:523
  2.6 0.0 copy-start
  2.6 1.2 %copy-done = bf16[1024,512]{1,0:T(8,128)(2,1)S(1)} copy-done((bf16[1024,512]{1,0:T(8,128)(2,1)S(1)}, bf16[1024,512]{1,0:T(8,128)(2,1)}, u32[]{:S(2)}) %copy-start) | copy-done | bytes 1048600
  3.8 83.2 %layer.1 = (bf16[768,2048]{1,0:T(8,128)(2,1)S(1)}, bf16[768,2048]{1,0:T(8,128)(2,1)S(1)}, bf16[768,2048]{1,0:T(8,128)(2,1)S(1)}, bf16[1024,512]{1,0:T(8,128)(2,1)S(1)}) custom-call(bf16[1024,512]{1,0:T(8,128)(2,1)S(1)} %copy-done, bf16[32,704]{1,0:T(8,128)(2,1)S(1)} %get-tuple-element.21.gw, bf16[32,704]{1,0:T(8,128)(2,1)S(1)} %get-tuple-element.20.uw, ...), custom_call_target="tpu_custom_call" | custom-call | tf_op jit(solution)/shard_map/layer/pallas_call | solution.py:488
  87.1 3.8 %hand_out.1 = (bf16[704,2048]{1,0:T(8,128)(2,1)}, bf16[704,2048]{1,0:T(8,128)(2,1)}, bf16[704,2048]{1,0:T(8,128)(2,1)}, bf16[1024,512]{1,0:T(8,128)(2,1)}) custom-call(bf16[768,2048]{1,0:T(8,128)(2,1)S(1)} %get-tuple-element.12.gt, bf16[768,2048]{1,0:T(8,128)(2,1)S(1)} %get-tuple-element.13.ut, bf16[768,2048]{1,0:T(8,128)(2,1)S(1)} %get-tuple-element.14.df, ...), custom_call_target="tpu_custom_call" | custom-call | tf_op jit(solution)/shard_map/hand_out/pallas_call | solution.py:526
Async XLA Ops:
  2.6 1.2 %copy-start = (bf16[1024,512]{1,0:T(8,128)(2,1)S(1)}, bf16[1024,512]{1,0:T(8,128)(2,1)}, u32[]{:S(2)}) copy-start(bf16[1024,512]{1,0:T(8,128)(2,1)} %tok.1) | copy-start | bytes 3145732

commit v5 on v4

--- a/solution.py
+++ b/solution.py
@@ -63,28 +63,6 @@
     def _():
         pl.semaphore_signal(barrier, inc=1, device_id=swap, device_id_type=MESH)
 
-    with jax.named_scope("meet"):
-        pl.semaphore_wait(barrier, 8 + moves.astype(jnp.int32))
-
-    def token_copy(way, j):
-        rows = pl.ds(j * PIECE, PIECE)
-        return remote(tok.at[rows], xs.at[y, rows], ts.at[way], tr.at[way * PIECES + j], (y_next, y_prev)[way])
-
-    def token_forward(way, j):
-        rows = pl.ds(j * PIECE + way * (PIECE // 2), PIECE // 2)
-        block = xs.at[(ym, yp)[way], rows]
-        return remote(block, block, tfs.at[way], tfr.at[way * PIECES + j], (y_next, y_prev)[way])
-
-    def token_pass(j):
-        for way in range(2):
-            token_copy(way, j).wait_recv()
-            token_forward(way, j).start()
-
-    for j in range(PIECES):
-        for way in range(2):
-            token_copy(way, j).start()
-    own_tokens.start()
-
     for ref, dst in ((uw, sud.at[z, x, c, 0]), (gw, sg.at[z, x, c])):
         for t in range(5):
             for r in range(2):
@@ -108,12 +86,34 @@
     def _():
         own_down(sud.at[z, x, c, 1])
 
+    with jax.named_scope("meet"):
+        pl.semaphore_wait(barrier, 8 + moves.astype(jnp.int32))
+
     change = remote(dsend, sud.at[pz, x, c, 1], ps.at[0], pr.at[0], swap)
 
     @pl.when(moves)
     def _():
         change.start()
 
+    def token_copy(way, j):
+        rows = pl.ds(j * PIECE, PIECE)
+        return remote(tok.at[rows], xs.at[y, rows], ts.at[way], tr.at[way * PIECES + j], (y_next, y_prev)[way])
+
+    def token_forward(way, j):
+        rows = pl.ds(j * PIECE + way * (PIECE // 2), PIECE // 2)
+        block = xs.at[(ym, yp)[way], rows]
+        return remote(block, block, tfs.at[way], tfr.at[way * PIECES + j], (y_next, y_prev)[way])
+
+    def token_pass(j):
+        for way in range(2):
+            token_copy(way, j).wait_recv()
+            token_forward(way, j).start()
+
+    for j in range(PIECES):
+        for way in range(2):
+            token_copy(way, j).start()
+    own_tokens.start()
+
     order = [0, 7, 1, 6, 2, 5, 3, 4]
     last = ((4, 3), (3, 4))
 
@@ -143,12 +143,12 @@
         block = sg.at[came(way, k), pl.ds(0, 2), c]
         return remote(block, block, gzs.at[way], gzr.at[(way * 4 + k) * 2 + h], (z_next, z_prev)[way])
 
-    def g_twin(o):
-        block = sg.at[(z + order[o]) % NZ, :, c]
+    def g_twin(o, e):
+        block = sg.at[(z + order[o]) % NZ, (x, xp, xm, x2)[e], c]
         return remote(block, block, ds_.at[2], dr.at[2], twin)
 
-    def ud_twin(q, o):
-        block = sud.at[(z + order[o]) % NZ, :, c, q]
+    def ud_twin(q, o, e):
+        block = sud.at[(z + order[o]) % NZ, (x, xp, xm, x2)[e], c, q]
         return remote(block, block, ds_.at[q], dr.at[q], twin)
 
     def twins(n):
@@ -175,8 +175,8 @@
                     if k < 3 or k == 3 and h == way:
                         for e in (2 * h, 2 * h + 1):
                             g_z(way, k, e).start()
-                    if h == 1:
-                        g_twin(place(way, k)).start()
+                    for e in (2 * h, 2 * h + 1):
+                        g_twin(place(way, k), e).start()
 
     def x_pass(q, *os):
         for o in os:
@@ -184,11 +184,13 @@
                 ud_x(q, o, way).wait_recv()
                 if way == q:
                     ud_f(q, o).start()
+            for e in range(3):
+                ud_twin(q, o, e).start()
 
     def x_end(q, *os):
         for o in os:
             ud_f(q, o).wait_recv()
-            ud_twin(q, o).start()
+            ud_twin(q, o, 3).start()
 
     def g_x(way):
         block = sg.at[z, x, c]
@@ -231,7 +233,8 @@
         shards_of(1, gxs.at[0], gxr.at[2]).wait_recv()
         for way in range(2):
             g_z(way, 0, 3).start()
-        g_twin(0).start()
+        for e in range(4):
+            g_twin(0, e).start()
     with jax.named_scope("round_2"):
         ud_round(0, 2)
         g_round(1, 0)
@@ -247,33 +250,30 @@
         x_pass(0, 3, 4)
         g_round(2, 1)
         x_pass(1, 1, 2)
-        x_end(0, 0)
+        x_end(0, 0, 1, 2)
+        x_end(1, 0)
     with jax.named_scope("round_4"):
         ud_round(0, 4)
         g_round(3, 0)
         ud_round(1, 3)
         x_pass(0, 5, 6)
         g_round(3, 1)
+        x_pass(0, 7)
         token_pass(1)
         x_pass(1, 3, 4)
-        x_end(0, 1, 2)
-        x_end(1, 0)
+        x_end(0, 3, 4)
     with jax.named_scope("round_5"):
         ud_round(1, 4)
-        x_pass(0, 7)
         g_round(4, 0, 1)
         token_pass(2)
-        x_end(0, 3, 4)
         x_pass(1, 5, 6)
+        x_end(0, 5, 6)
         x_end(1, 1, 2)
     with jax.named_scope("round_6"):
-        x_end(0, 5, 6)
         x_pass(1, 7)
         token_pass(3)
+        x_end(0, 7)
         x_end(1, 3, 4)
-    with jax.named_scope("round_7"):
-        x_end(0, 7)
-        x_end(1, 5, 6)
     own_tokens.wait()
 
     def normalise(j):
@@ -312,8 +312,8 @@
             halves.append(half.reshape(rows, 128))
         return jnp.concatenate(halves, axis=1)
 
-    def first():
-        for n in range(3):
+    def first(ns):
+        for n in ns:
             gate = jnp.dot(xn[...], columns(1, n, pl.ds(0, 4)), preferred_element_type=F32)
             up = jnp.dot(xn[...], columns(0, n, pl.ds(0, 4)), preferred_element_type=F32)
             hid[:, pl.ds(256 * n, 256)] = (gate / (1.0 + jnp.exp(-gate)) * up).astype(BF)
@@ -366,15 +366,25 @@
         for way in range(2):
             message("comb", way, j).start()
 
+    @pl.when(c == 1)
+    def _():
+        x_end(1, 5, 6, 7)
+
     with jax.named_scope("normalise_0"):
         normalise(0)
     with jax.named_scope("wait_up"):
-        x_end(1, 7)
         twins(2).wait_recv()
         twins(0).wait_recv()
     with jax.named_scope("first_0"):
         lax.fori_loop(0, NZ, spread, 0)
-        first()
+        first(range(3))
+
+    with jax.named_scope("last_down"):
+
+        @pl.when(c == 0)
+        def _():
+            x_end(1, 5, 6, 7)
+
     with jax.named_scope("wait_down"):
         twins(1).wait_recv()
 
@@ -424,7 +434,7 @@
         def _():
             with jax.named_scope("first"):
                 normalise(j + 1)
-                first()
+                first(range(3))
 
         @pl.when(jnp.logical_and(j >= 3, j < 7))
         def _():

time: 91 us -> 90.4 us (level)
  no operation moved by 1% of the time
where the time goes in v5:
time: 90.4 us; the launch traced here: 90.3 us
  Pallas kernels  86.4 us (96%)
  other arithmetic  1.94 us (2%)
  local copies, waits for them, and re-layouts  1.22 us (1%)
    pallas_call x1, Pallas kernels, shards(): pl.pallas_call(kernel, name='layer', out_shape=(jax.ShapeDtypeStruct((WID...  82.7 us
    pallas_call x1, Pallas kernels, shards(): pl.pallas_call(hand_out, name='hand_out', out_shape=(jax.ShapeDtypeStruct...  3.77 us

profile of v5, /device:TPU:1, one launch (start us, length us, event | category | flops | bytes accessed | tf_op | source)
XLA Modules:
  0.0 90.3 jit_solution(9604607393573833670)
XLA Ops:
  0.6 0.9 convert_element_type.11.dw
  1.5 1.0 %multiply_convert_fusion = (bf16[32,704]{1,0:T(8,128)(2,1)S(1)}, bf16[32,704]{1,0:T(8,128)(2,1)S(1)}) fusion(f32[32,704]{1,0:T(8,128)} %param.8, f32[32]{0:T(128)} %param.6, f32[32,704]{1,0:T(8,128)} %param.7), kind=kLoop, calls=%fused_computation | loop fusion | flops 90112 | bytes 270464 | tf_op jit(solution)/shard_map/convert_element_type | solution.py:533
  2.6 0.0 copy-start
  2.6 1.2 %copy-done = bf16[1024,512]{1,0:T(8,128)(2,1)S(1)} copy-done((bf16[1024,512]{1,0:T(8,128)(2,1)S(1)}, bf16[1024,512]{1,0:T(8,128)(2,1)}, u32[]{:S(2)}) %copy-start) | copy-done | bytes 1048600
  3.8 82.7 %layer.1 = (bf16[768,2048]{1,0:T(8,128)(2,1)S(1)}, bf16[768,2048]{1,0:T(8,128)(2,1)S(1)}, bf16[768,2048]{1,0:T(8,128)(2,1)S(1)}, bf16[1024,512]{1,0:T(8,128)(2,1)S(1)}) custom-call(bf16[1024,512]{1,0:T(8,128)(2,1)S(1)} %copy-done, bf16[32,704]{1,0:T(8,128)(2,1)S(1)} %get-tuple-element.21.gw, bf16[32,704]{1,0:T(8,128)(2,1)S(1)} %get-tuple-element.20.uw, ...), custom_call_target="tpu_custom_call" | custom-call | tf_op jit(solution)/shard_map/layer/pallas_call | solution.py:498
  86.5 3.8 %hand_out.1 = (bf16[704,2048]{1,0:T(8,128)(2,1)}, bf16[704,2048]{1,0:T(8,128)(2,1)}, bf16[704,2048]{1,0:T(8,128)(2,1)}, bf16[1024,512]{1,0:T(8,128)(2,1)}) custom-call(bf16[768,2048]{1,0:T(8,128)(2,1)S(1)} %get-tuple-element.12.gt, bf16[768,2048]{1,0:T(8,128)(2,1)S(1)} %get-tuple-element.13.ut, bf16[768,2048]{1,0:T(8,128)(2,1)S(1)} %get-tuple-element.14.df, ...), custom_call_target="tpu_custom_call" | custom-call | tf_op jit(solution)/shard_map/hand_out/pallas_call | solution.py:536
Async XLA Ops:
  2.6 1.2 %copy-start = (bf16[1024,512]{1,0:T(8,128)(2,1)S(1)}, bf16[1024,512]{1,0:T(8,128)(2,1)}, u32[]{:S(2)}) copy-start(bf16[1024,512]{1,0:T(8,128)(2,1)} %tok.1) | copy-start | bytes 3145732

commit v6 on v5

--- a/solution.py
+++ b/solution.py
@@ -28,7 +28,7 @@
     tok, gw, uw, dw,
     gt, ut, df, out,
     xs, sg, sud, ends, dsend, tmp, xn, hid, part, far, got, sums,
-    ps, pr, gxs, gxr, gzs, gzr, us, ur, uxs, uxr, ufs, ufr, ds_, dr, ts, tr, tfs, tfr, rs, rr, loc,
+    ps, pr, gxs, gxr, gzs, gzr, us, ur, uxs, uxr, ufs, ufr, ds_, dr, ts, tr, tfs, tfr, rs, rr, zfs, zfr, loc,
 ):
     f, y = lax.axis_index("fs"), lax.axis_index("tp")
     z, x, c = f // 8, (f // 2) % 4, f % 2
@@ -43,7 +43,7 @@
     z_next, z_prev = at(zp, x, c, y), at(zm, x, c, y)
     x_next, x_prev, x_far = at(z, xp, c, y), at(z, xm, c, y), at(z, x2, c, y)
     y_next, y_prev = at(z, x, c, yp), at(z, x, c, ym)
-    twin = at(z, x, 1 - c, y)
+    twin, z_far = at(z, x, 1 - c, y), at((z + 4) % NZ, x, c, y)
     pz = 2 * y + zb
     swap = at(pz, x, c, za)
     moves = za != y
@@ -56,7 +56,7 @@
     own_tokens = pltpu.make_async_copy(tok, xs.at[y], loc.at[0])
 
     barrier = pltpu.get_barrier_semaphore()
-    for partner in (z_next, z_prev, x_next, x_prev, x_far, y_next, y_prev, twin):
+    for partner in (z_next, z_prev, z_far, x_next, x_prev, y_next, y_prev, twin):
         pl.semaphore_signal(barrier, inc=1, device_id=partner, device_id_type=MESH)
 
     @pl.when(moves)
@@ -115,7 +115,7 @@
     own_tokens.start()
 
     order = [0, 7, 1, 6, 2, 5, 3, 4]
-    last = ((4, 3), (3, 4))
+    last = ((3, 3), (3, 4))
 
     def came(way, k):
         return (z + (NZ - k if way == 0 else k)) % NZ
@@ -204,11 +204,14 @@
         block = sg.at[z, pl.ds(0, n), c]
         return remote(block, block, send, recv, x_next)
 
+    own_up = sud.at[z, x, c, 0]
+    far_up = remote(own_up, own_up, zfs.at[0], zfr.at[0], z_far)
     for way in range(2):
         ud_z(0, way, 0).start()
     for way in range(2):
         g_x(way).start()
     ud_arrived(0, 0)
+    far_up.start()
     for way in range(2):
         g_z(way, 0, 0).start()
 
@@ -230,6 +233,8 @@
             for way in range(2):
                 g_z(way, 0, e).start()
         x_pass(0, 0)
+        far_up.wait_recv()
+        ud_arrived(0, 7)
         shards_of(1, gxs.at[0], gxr.at[2]).wait_recv()
         for way in range(2):
             g_z(way, 0, 3).start()
@@ -239,7 +244,7 @@
         ud_round(0, 2)
         g_round(1, 0)
         ud_round(1, 1)
-        x_pass(0, 1, 2)
+        x_pass(0, 1, 2, 7)
         g_round(1, 1)
         x_pass(1, 0)
         token_pass(0)
@@ -253,15 +258,13 @@
         x_end(0, 0, 1, 2)
         x_end(1, 0)
     with jax.named_scope("round_4"):
-        ud_round(0, 4)
         g_round(3, 0)
         ud_round(1, 3)
         x_pass(0, 5, 6)
         g_round(3, 1)
-        x_pass(0, 7)
         token_pass(1)
         x_pass(1, 3, 4)
-        x_end(0, 3, 4)
+        x_end(0, 7, 3, 4)
     with jax.named_scope("round_5"):
         ud_round(1, 4)
         g_round(4, 0, 1)
@@ -272,7 +275,6 @@
     with jax.named_scope("round_6"):
         x_pass(1, 7)
         token_pass(3)
-        x_end(0, 7)
         x_end(1, 3, 4)
     own_tokens.wait()
 
@@ -463,8 +465,9 @@
             change.wait_send()
 
         shards_of(3, gxs.at[0], gxr.at[0]).wait_send()
-        for way in range(2):
-            block = sg.at[pl.ds(0, 7), x, c]
+        far_up.wait_send()
+        for way in range(2):
+            block = sg.at[pl.ds(0, (6, 7)[way]), x, c]
             remote(block, block, us.at[way], ur.at[0], z_next).wait_send()
             block = sg.at[pl.ds(0, 7), x]
             remote(block, block, gzs.at[way], gzr.at[0], z_next).wait_send()
@@ -524,6 +527,7 @@
             sem((2,)), sem((2 * PIECES,)),
             sem((2,)), sem((2 * PIECES,)),
             sem((1,)), sem((2 * CHUNKS,)),
+            sem((1,)), sem((1,)),
             sem((1,)),
         ],
         compiler_params=pltpu.CompilerParams(collective_id=0, has_side_effects=True, vmem_limit_bytes=LIMIT),

time: 90.4 us -> 89.7 us (level)
  no operation moved by 1% of the time
where the time goes in v6:
time: 89.7 us; the launch traced here: 89.5 us
  Pallas kernels  85.7 us (96%)
  other arithmetic  1.94 us (2%)
  local copies, waits for them, and re-layouts  1.22 us (1%)
    pallas_call x1, Pallas kernels, shards(): pl.pallas_call(kernel, name='layer', out_shape=(jax.ShapeDtypeStruct((WID...  81.9 us
    pallas_call x1, Pallas kernels, shards(): pl.pallas_call(hand_out, name='hand_out', out_shape=(jax.ShapeDtypeStruct...  3.77 us

profile of v6, /device:TPU:1, one launch (start us, length us, event | category | flops | bytes accessed | tf_op | source)
XLA Modules:
  0.0 89.5 jit_solution(15320937141656259588)
XLA Ops:
  0.6 0.9 %convert_element_type.11.dw = bf16[44,512]{1,0:T(8,128)(2,1)S(1)} convert(f32[44,512]{1,0:T(8,128)} %param.9) | non-fusion elementwise | flops 22528 | bytes 135168 | tf_op jit(solution)/shard_map/convert_element_type | solution.py:538
  1.5 1.0 %multiply_convert_fusion = (bf16[32,704]{1,0:T(8,128)(2,1)S(1)}, bf16[32,704]{1,0:T(8,128)(2,1)S(1)}) fusion(f32[32,704]{1,0:T(8,128)} %param.8, f32[32]{0:T(128)} %param.6, f32[32,704]{1,0:T(8,128)} %param.7), kind=kLoop, calls=%fused_computation | loop fusion | flops 90112 | bytes 270464 | tf_op jit(solution)/shard_map/convert_element_type | solution.py:537
  2.6 0.0 copy-start
  2.6 1.2 %copy-done = bf16[1024,512]{1,0:T(8,128)(2,1)S(1)} copy-done((bf16[1024,512]{1,0:T(8,128)(2,1)S(1)}, bf16[1024,512]{1,0:T(8,128)(2,1)}, u32[]{:S(2)}) %copy-start) | copy-done | bytes 1048600
  3.8 81.9 %layer.1 = (bf16[768,2048]{1,0:T(8,128)(2,1)S(1)}, bf16[768,2048]{1,0:T(8,128)(2,1)S(1)}, bf16[768,2048]{1,0:T(8,128)(2,1)S(1)}, bf16[1024,512]{1,0:T(8,128)(2,1)S(1)}) custom-call(bf16[1024,512]{1,0:T(8,128)(2,1)S(1)} %copy-done, bf16[32,704]{1,0:T(8,128)(2,1)S(1)} %get-tuple-element.21.gw, bf16[32,704]{1,0:T(8,128)(2,1)S(1)} %get-tuple-element.20.uw, ...), custom_call_target="tpu_custom_call" | custom-call | tf_op jit(solution)/shard_map/layer/pallas_call | solution.py:501
  85.7 3.8 %hand_out.1 = (bf16[704,2048]{1,0:T(8,128)(2,1)}, bf16[704,2048]{1,0:T(8,128)(2,1)}, bf16[704,2048]{1,0:T(8,128)(2,1)}, bf16[1024,512]{1,0:T(8,128)(2,1)}) custom-call(bf16[768,2048]{1,0:T(8,128)(2,1)S(1)} %get-tuple-element.12.gt, bf16[768,2048]{1,0:T(8,128)(2,1)S(1)} %get-tuple-element.13.ut, bf16[768,2048]{1,0:T(8,128)(2,1)S(1)} %get-tuple-element.14.df, ...), custom_call_target="tpu_custom_call" | custom-call | tf_op jit(solution)/shard_map/hand_out/pallas_call | solution.py:540
Async XLA Ops:
  2.6 1.2 %copy-start = (bf16[1024,512]{1,0:T(8,128)(2,1)S(1)}, bf16[1024,512]{1,0:T(8,128)(2,1)}, u32[]{:S(2)}) copy-start(bf16[1024,512]{1,0:T(8,128)(2,1)} %tok.1) | copy-start | bytes 3145732

commit v7 on v6

--- a/solution.py
+++ b/solution.py
@@ -27,7 +27,7 @@
 def kernel(
     tok, gw, uw, dw,
     gt, ut, df, out,
-    xs, sg, sud, ends, dsend, tmp, xn, hid, part, far, got, sums,
+    xs, sg, sud, ends, dsend, tmp, xn, hid, part, faraway, got, sums,
     ps, pr, gxs, gxr, gzs, gzr, us, ur, uxs, uxr, ufs, ufr, ds_, dr, ts, tr, tfs, tfr, rs, rr, zfs, zfr, loc,
 ):
     f, y = lax.axis_index("fs"), lax.axis_index("tp")
@@ -115,7 +115,7 @@
     own_tokens.start()
 
     order = [0, 7, 1, 6, 2, 5, 3, 4]
-    last = ((3, 3), (3, 4))
+    last = ((3, 3), (3, 3))
 
     def came(way, k):
         return (z + (NZ - k if way == 0 else k)) % NZ
@@ -170,9 +170,9 @@
     def g_round(k, *hs):
         for h in hs:
             for way in range(2):
-                if k < 4 or h == way:
+                if k < 4 or way == 1:
                     g_pair(way, k - 1, h).wait_recv()
-                    if k < 3 or k == 3 and h == way:
+                    if k < 3 or k == 3 and way == 1:
                         for e in (2 * h, 2 * h + 1):
                             g_z(way, k, e).start()
                     for e in (2 * h, 2 * h + 1):
@@ -204,14 +204,16 @@
         block = sg.at[z, pl.ds(0, n), c]
         return remote(block, block, send, recv, x_next)
 
-    own_up = sud.at[z, x, c, 0]
-    far_up = remote(own_up, own_up, zfs.at[0], zfr.at[0], z_far)
+    def far(q):
+        block = sud.at[z, x, c, q]
+        return remote(block, block, zfs.at[q], zfr.at[q], z_far)
+
     for way in range(2):
         ud_z(0, way, 0).start()
     for way in range(2):
         g_x(way).start()
     ud_arrived(0, 0)
-    far_up.start()
+    far(0).start()
     for way in range(2):
         g_z(way, 0, 0).start()
 
@@ -223,6 +225,7 @@
 
     for way in range(2):
         ud_z(1, way, 0).start()
+    far(1).start()
     ud_arrived(1, 0)
     with jax.named_scope("round_1"):
         for way in range(2):
@@ -233,7 +236,7 @@
             for way in range(2):
                 g_z(way, 0, e).start()
         x_pass(0, 0)
-        far_up.wait_recv()
+        far(0).wait_recv()
         ud_arrived(0, 7)
         shards_of(1, gxs.at[0], gxr.at[2]).wait_recv()
         for way in range(2):
@@ -245,6 +248,8 @@
         g_round(1, 0)
         ud_round(1, 1)
         x_pass(0, 1, 2, 7)
+        far(1).wait_recv()
+        ud_arrived(1, 7)
         g_round(1, 1)
         x_pass(1, 0)
         token_pass(0)
@@ -254,7 +259,7 @@
         ud_round(1, 2)
         x_pass(0, 3, 4)
         g_round(2, 1)
-        x_pass(1, 1, 2)
+        x_pass(1, 1, 2, 7)
         x_end(0, 0, 1, 2)
         x_end(1, 0)
     with jax.named_scope("round_4"):
@@ -266,14 +271,12 @@
         x_pass(1, 3, 4)
         x_end(0, 7, 3, 4)
     with jax.named_scope("round_5"):
-        ud_round(1, 4)
         g_round(4, 0, 1)
         token_pass(2)
         x_pass(1, 5, 6)
         x_end(0, 5, 6)
-        x_end(1, 1, 2)
+        x_end(1, 1, 2, 7)
     with jax.named_scope("round_6"):
-        x_pass(1, 7)
         token_pass(3)
         x_end(1, 3, 4)
     own_tokens.wait()
@@ -334,11 +337,11 @@
         rows = {"far": 1 - way, "near": way, "comb": 1 - way}[kind]
         to_block = y2 if kind == "far" else (yp, ym)[way]
         src = sums.at[j, way] if kind == "comb" else part.at[j, to_block, pl.ds(rows * HALF, HALF)]
-        dst = {"far": far.at[j, way], "near": got.at[j, way], "comb": got.at[j, 2 + way]}[kind]
+        dst = {"far": faraway.at[j, way], "near": got.at[j, way], "comb": got.at[j, 2 + way]}[kind]
         return remote(src, dst, rs.at[0], rr.at[j + (0 if kind == "far" else CHUNKS)], (y_next, y_prev)[way])
 
     def all_far(j):
-        return remote(sums.at[j], far.at[j], rs.at[0], rr.at[j], y_next)
+        return remote(sums.at[j], faraway.at[j], rs.at[0], rr.at[j], y_next)
 
     def all_got(j):
         return remote(got.at[j], got.at[j], rs.at[0], rr.at[CHUNKS + j], y_next)
@@ -364,13 +367,13 @@
         all_far(j).wait_recv()
         for way in range(2):
             mine = part[j, (yp, ym)[way], pl.ds((1 - way) * HALF, HALF), :].astype(F32)
-            sums[j, way] = (mine + far[j, way].astype(F32)).astype(BF)
+            sums[j, way] = (mine + faraway[j, way].astype(F32)).astype(BF)
         for way in range(2):
             message("comb", way, j).start()
 
     @pl.when(c == 1)
     def _():
-        x_end(1, 5, 6, 7)
+        x_end(1, 5, 6)
 
     with jax.named_scope("normalise_0"):
         normalise(0)
@@ -385,7 +388,7 @@
 
         @pl.when(c == 0)
         def _():
-            x_end(1, 5, 6, 7)
+            x_end(1, 5, 6)
 
     with jax.named_scope("wait_down"):
         twins(1).wait_recv()
@@ -465,11 +468,12 @@
             change.wait_send()
 
         shards_of(3, gxs.at[0], gxr.at[0]).wait_send()
-        far_up.wait_send()
-        for way in range(2):
-            block = sg.at[pl.ds(0, (6, 7)[way]), x, c]
+        for q in range(2):
+            far(q).wait_send()
+        for way in range(2):
+            block = sg.at[pl.ds(0, 6), x, c]
             remote(block, block, us.at[way], ur.at[0], z_next).wait_send()
-            block = sg.at[pl.ds(0, 7), x]
+            block = sg.at[pl.ds(0, (6, 8)[way]), x]
             remote(block, block, gzs.at[way], gzr.at[0], z_next).wait_send()
             remote(tok, xs.at[y], ts.at[way], tr.at[0], y_next).wait_send()
             half = xs.at[0, pl.ds(0, PIECE * PIECES // 2)]
@@ -527,7 +531,7 @@
             sem((2,)), sem((2 * PIECES,)),
             sem((2,)), sem((2 * PIECES,)),
             sem((1,)), sem((2 * CHUNKS,)),
-            sem((1,)), sem((1,)),
+            sem((2,)), sem((2,)),
             sem((1,)),
         ],
         compiler_params=pltpu.CompilerParams(collective_id=0, has_side_effects=True, vmem_limit_bytes=LIMIT),

time: 89.7 us -> 89.6 us (level)
  no operation moved by 1% of the time
where the time goes in v7:
time: 89.6 us; the launch traced here: 89.4 us
  Pallas kernels  85.6 us (96%)
  other arithmetic  1.94 us (2%)
  local copies, waits for them, and re-layouts  1.22 us (1%)
    pallas_call x1, Pallas kernels, shards(): pl.pallas_call(kernel, name='layer', out_shape=(jax.ShapeDtypeStruct((WID...  81.8 us
    pallas_call x1, Pallas kernels, shards(): pl.pallas_call(hand_out, name='hand_out', out_shape=(jax.ShapeDtypeStruct...  3.77 us

profile of v7, /device:TPU:1, one launch (start us, length us, event | category | flops | bytes accessed | tf_op | source)
XLA Modules:
  0.0 89.4 jit_solution(15384765582776055473)
XLA Ops:
  0.6 0.9 %convert_element_type.11.dw = bf16[44,512]{1,0:T(8,128)(2,1)S(1)} convert(f32[44,512]{1,0:T(8,128)} %param.9) | non-fusion elementwise | flops 22528 | bytes 135168 | tf_op jit(solution)/shard_map/convert_element_type | solution.py:542
  1.5 1.0 %multiply_convert_fusion = (bf16[32,704]{1,0:T(8,128)(2,1)S(1)}, bf16[32,704]{1,0:T(8,128)(2,1)S(1)}) fusion(f32[32,704]{1,0:T(8,128)} %param.8, f32[32]{0:T(128)} %param.6, f32[32,704]{1,0:T(8,128)} %param.7), kind=kLoop, calls=%fused_computation | loop fusion | flops 90112 | bytes 270464 | tf_op jit(solution)/shard_map/convert_element_type | solution.py:541
  2.6 0.0 copy-start
  2.6 1.2 %copy-done = bf16[1024,512]{1,0:T(8,128)(2,1)S(1)} copy-done((bf16[1024,512]{1,0:T(8,128)(2,1)S(1)}, bf16[1024,512]{1,0:T(8,128)(2,1)}, u32[]{:S(2)}) %copy-start) | copy-done | bytes 1048600
  3.8 81.8 %layer.1 = (bf16[768,2048]{1,0:T(8,128)(2,1)S(1)}, bf16[768,2048]{1,0:T(8,128)(2,1)S(1)}, bf16[768,2048]{1,0:T(8,128)(2,1)S(1)}, bf16[1024,512]{1,0:T(8,128)(2,1)S(1)}) custom-call(bf16[1024,512]{1,0:T(8,128)(2,1)S(1)} %copy-done, bf16[32,704]{1,0:T(8,128)(2,1)S(1)} %get-tuple-element.21.gw, bf16[32,704]{1,0:T(8,128)(2,1)S(1)} %get-tuple-element.20.uw, ...), custom_call_target="tpu_custom_call" | custom-call | tf_op jit(solution)/shard_map/layer/pallas_call | solution.py:505
  85.6 3.8 %hand_out.1 = (bf16[704,2048]{1,0:T(8,128)(2,1)}, bf16[704,2048]{1,0:T(8,128)(2,1)}, bf16[704,2048]{1,0:T(8,128)(2,1)}, bf16[1024,512]{1,0:T(8,128)(2,1)}) custom-call(bf16[768,2048]{1,0:T(8,128)(2,1)S(1)} %get-tuple-element.12.gt, bf16[768,2048]{1,0:T(8,128)(2,1)S(1)} %get-tuple-element.13.ut, bf16[768,2048]{1,0:T(8,128)(2,1)S(1)} %get-tuple-element.14.df, ...), custom_call_target="tpu_custom_call" | custom-call | tf_op jit(solution)/shard_map/hand_out/pallas_call | solution.py:544
Async XLA Ops:
  2.6 1.2 %copy-start = (bf16[1024,512]{1,0:T(8,128)(2,1)S(1)}, bf16[1024,512]{1,0:T(8,128)(2,1)}, u32[]{:S(2)}) copy-start(bf16[1024,512]{1,0:T(8,128)(2,1)} %tok.1) | copy-start | bytes 3145732
